TPU v7x, 32 devices: a whole 2x2x4 slice. The times are simulated.
32 devices in a mesh: kv: 16 (over z, y, x), tp: 2 (over core).
Axes of the slice: x: 2, y: 2, z: 4, core: 2. Of those that a mesh axis runs over, the one named last changes fastest.
Arguments:
- tokens: bfloat16 [64, 4, 2048], P('kv', None, 'tp'), may hold values from -6 to 6
- input_gain: float32 [2048], replicated, may hold values from 0.1 to 1.9
- gate_weight: bfloat16 [2048, 4096], P('kv', 'tp'), may hold values from -0.125 to 0.125
- value_weight: bfloat16 [2048, 4096], P('kv', 'tp'), may hold values from -0.125 to 0.125
- write_weight: bfloat16 [2048, 1024], P('kv', 'tp'), may hold values from -0.125 to 0.125
- read_weight: bfloat16 [2048, 1024], P('kv', 'tp'), may hold values from -0.125 to 0.125
- step_weight: bfloat16 [2048, 64], replicated, may hold values from -0.125 to 0.125
- conv_value: float32 [4, 4096], P(None, 'tp'), may hold values from -3 to 3
- conv_write: float32 [4, 1024], P(None, 'tp'), may hold values from -3 to 3
- conv_read: float32 [4, 1024], P(None, 'tp'), may hold values from -3 to 3
- step_bias: float32 [64], P('tp'), may hold values from -4 to -1
- decay_log: float32 [64], P('tp'), may hold values from 0 to 2.8
- skip_gain: float32 [64], P('tp'), may hold values from 0.5 to 1.5
- output_gain: float32 [4096], P('tp'), may hold values from 0.1 to 1.9
- out_weight: bfloat16 [4096, 2048], P('tp', 'kv'), may hold values from -0.09375 to 0.09375
- base_state: float32 [64, 64, 64, 128], P('kv', 'tp'), may hold values from -2 to 2
- past_value: bfloat16 [64, 7, 4096], P('kv', None, 'tp'), may hold values from -6 to 6
- past_write: bfloat16 [64, 7, 1024], P('kv', None, 'tp'), may hold values from -6 to 6
- past_read: bfloat16 [64, 7, 1024], P('kv', None, 'tp'), may hold values from -6 to 6
- past_step: bfloat16 [64, 4, 64], P('kv', None, 'tp'), may hold values from -4 to 4
- accepted: int32 [64], P('kv'), may hold values from 1 to 4
Outputs:
- mixed: bfloat16 [64, 4, 2048], P('kv', None, 'tp')
- root_state: float32 [64, 64, 64, 128], P('kv', 'tp')
- next_value: bfloat16 [64, 7, 4096], P('kv', None, 'tp')
- next_write: bfloat16 [64, 7, 1024], P('kv', None, 'tp')
- next_read: bfloat16 [64, 7, 1024], P('kv', None, 'tp')
- next_step: bfloat16 [64, 4, 64], P('kv', None, 'tp')
Inputs may be any that keep to these rules, and one draw needn't show every extreme that they name: Every entry of `accepted` is an integer from 1 to 4 (at least one of the last step's proposals is always accepted).
All inputs are finite; a program needn't handle non-finite values.
Results may differ from a plain program's by a relative error of at most 0.018.
Values may be sent and summed in bfloat16 or wider, within the bound.
No kernel may reach another device: no remote copies, remote signals or barrier semaphores. Data moves between devices by JAX's collectives and lax.ppermute only.
A program may use at most 64 MiB of HBM per device.

v0:
```python
import functools

import jax
import jax.numpy as jnp
from jax import lax
from jax.experimental import pallas as pl
from jax.experimental.pallas import tpu as pltpu
from jax.sharding import PartitionSpec as P


CONV_W = 4
EPSILON = 1e-06


def silu(v):
    return v / (1.0 + jnp.exp(-v))


def softplus(v):
    return jnp.maximum(v, 0.0) + jnp.log1p(jnp.exp(-jnp.abs(v)))


def spread(heads, width):
    lane = lax.broadcasted_iota(jnp.int32, (heads, heads * width), 1)
    head = lax.broadcasted_iota(jnp.int32, (heads, heads * width), 0)
    return jnp.where(lane // width == head, 1.0, 0.0)


def halves_of(item):
    high = item.astype(jnp.bfloat16).astype(jnp.float32)
    return high, item - high


def grant(mib):
    return pltpu.CompilerParams(vmem_limit_bytes=mib * 1024 * 1024)


def turned(item):
    return (item.shape[1], item.shape[0]) + item.shape[2:]


def close(item):
    return pltpu.with_memory_space_constraint(item, pltpu.VMEM)


def pack_kernel(inner, spans, gate_ref, value_ref, write_ref, read_ref, *refs):
    outs, sems = refs[:inner], refs[inner]
    me = lax.rem(lax.axis_index("kv"), inner)
    copies = []
    for step in range(inner):
        target, low = me ^ step, 0
        for kind, ref in enumerate((gate_ref, value_ref, write_ref, read_ref)):
            span = spans[kind]
            first = pl.multiple_of(target * span, span)
            copies.append(
                pltpu.make_async_copy(
                    ref.at[:, pl.ds(first, span)],
                    outs[step].at[:, low : low + span],
                    sems.at[step * 4 + kind],
                )
            )
            low = low + span
    for copy in copies:
        copy.start()
    for copy in copies:
        copy.wait()


def make_packed(weights, spans, inner):
    depth = weights[0].shape[0]
    return pl.pallas_call(
        functools.partial(pack_kernel, inner, spans),
        in_specs=[pl.BlockSpec(memory_space=pltpu.HBM)] * 4,
        out_specs=[pl.BlockSpec(memory_space=pltpu.VMEM)] * inner,
        out_shape=[pltpu.VMEM((depth, sum(spans)), jnp.bfloat16)] * inner,
        scratch_shapes=[pltpu.SemaphoreType.DMA((4 * inner,))],
        compiler_params=grant(4),
        name="pack",
    )(*[pltpu.with_memory_space_constraint(item, pltpu.HBM) for item in weights])


def partial_kernel(inner, rows_ref, *refs):
    weights, out_ref = refs[:inner], refs[inner]
    depth = weights[0].shape[0]
    me = lax.rem(lax.axis_index("kv"), inner)
    total = None
    for step in range(inner):
        first = pl.multiple_of((me ^ step) * depth, depth)
        term = jnp.dot(
            rows_ref[:, pl.ds(first, depth)],
            weights[step][...],
            preferred_element_type=jnp.float32,
        )
        total = term if total is None else total + term
    out_ref[...] = total.astype(jnp.bfloat16)


def make_partial(rows, weights):
    count, width = rows.shape[0], weights[0].shape[1]
    vmem = pl.BlockSpec(memory_space=pltpu.VMEM)
    return pl.pallas_call(
        functools.partial(partial_kernel, len(weights)),
        in_specs=[vmem] * (1 + len(weights)),
        out_specs=vmem,
        out_shape=pltpu.VMEM((count, width), jnp.bfloat16),
        cost_estimate=pl.CostEstimate(
            flops=2 * rows.size * width, bytes_accessed=2 * count * width, transcendentals=0
        ),
        compiler_params=grant(12),
        name="partial",
    )(close(rows), *[close(item) for item in weights])


def root_kernel(
    taken_ref,
    base_ref,
    past_x_ref,
    past_b_ref,
    past_dt_ref,
    conv_x_ref,
    conv_b_ref,
    bias_ref,
    decay_ref,
    root_ref,
    short_ref,
):
    _, heads, width, states = base_ref.shape
    steps = past_dt_ref.shape[1]
    groups = past_b_ref.shape[2] // states
    span = heads * width // groups
    taken = taken_ref[pl.program_id(0)]
    copies = spread(heads, width)
    fixed = jnp.dot(
        jnp.concatenate([bias_ref[...], decay_ref[...]], axis=0),
        copies,
        precision=lax.Precision.HIGHEST,
        preferred_element_type=jnp.float32,
    )
    step = jnp.dot(
        past_dt_ref[0], copies.astype(jnp.bfloat16), preferred_element_type=jnp.float32
    )
    dt = softplus(step + fixed[0:1])
    live = lax.broadcasted_iota(jnp.int32, dt.shape, 0) < taken
    logs = jnp.where(live, -jnp.exp(fixed[1:2]) * dt, 0.0)
    tails = [jnp.zeros_like(logs[0:1])]
    for row in range(steps - 1, 0, -1):
        tails.insert(0, tails[0] + logs[row : row + 1])
    total = tails[0] + logs[0:1]
    weight = jnp.where(live, jnp.exp(jnp.concatenate(tails, axis=0)) * dt, 0.0)

    def conv(rows, taps):
        return sum(taps[k : k + 1] * rows[k : k + steps] for k in range(CONV_W))

    left = weight * silu(conv(past_x_ref[0].astype(jnp.float32), conv_x_ref[...]))
    right = silu(conv(past_b_ref[0].astype(jnp.float32), conv_b_ref[...]))
    left_high, left_low = halves_of(left)
    right_high, right_low = halves_of(right)
    scale = jnp.exp(total)
    scale_high, rest = halves_of(scale)
    scale_mid, rest = halves_of(rest)
    lhs = jnp.concatenate(
        [left_high, left_high, left_low, scale_high, scale_mid, rest, jnp.zeros_like(rest)], axis=0
    ).astype(jnp.bfloat16)
    rhs = jnp.concatenate([right_high, right_low, right_high], axis=0)
    rhs = jnp.concatenate([rhs, jnp.zeros((4, rhs.shape[1]), jnp.float32)], axis=0).astype(
        jnp.bfloat16
    )
    row = lax.broadcasted_iota(jnp.int32, (3 * steps + 4, states), 0)
    ones = jnp.where((row >= 3 * steps) & (row < 3 * steps + 3), 1.0, 0.0).astype(jnp.bfloat16)
    each = heads // groups
    for group in range(groups):
        both = lax.dot_general(
            lhs[:, group * span : (group + 1) * span],
            jnp.concatenate([rhs[:, group * states : (group + 1) * states], ones], axis=1),
            (((0,), (0,)), ((), ())),
            preferred_element_type=jnp.float32,
        )
        base = base_ref[0, group * each : (group + 1) * each].reshape(span, states)
        root = both[:, states:] * base + both[:, :states]
        root_ref[0, group * each : (group + 1) * each] = root.reshape(each, width, states)
        short_ref[0, group * span : (group + 1) * span] = root.astype(jnp.bfloat16)


def make_root(base, past_x, past_b, past_dt, taken, conv_x, conv_b, bias, decay):
    count, heads, width, states = base.shape

    def one(*dims):
        return pl.BlockSpec((1,) + dims, lambda s: (s,) + (0,) * len(dims))

    def same(item):
        return pl.BlockSpec(item.shape, lambda s: (0,) * item.ndim)

    args = (past_x, past_b, past_dt)
    fixed = (conv_x, conv_b, bias[None], decay[None])
    return pl.pallas_call(
        root_kernel,
        grid=(count,),
        in_specs=[pl.BlockSpec(memory_space=pltpu.SMEM), one(*base.shape[1:])]
        + [one(*item.shape[1:]) for item in args]
        + [same(item) for item in fixed],
        out_specs=[one(*base.shape[1:]), one(heads * width, states)],
        out_shape=[
            jax.ShapeDtypeStruct(base.shape, jnp.float32),
            jax.ShapeDtypeStruct((count, heads * width, states), jnp.bfloat16),
        ],
        cost_estimate=pl.CostEstimate(
            flops=4 * base.size * 16, bytes_accessed=10 * base.size, transcendentals=0
        ),
        compiler_params=grant(16),
        name="root",
    )(taken, base, *args, *fixed)


def mixer_kernel(
    outer,
    inner,
    spans,
    taken_ref,
    parts_ref,
    short_ref,
    step_ref,
    past_x_ref,
    past_b_ref,
    past_c_ref,
    conv_x_ref,
    conv_b_ref,
    conv_c_ref,
    bias_ref,
    decay_ref,
    skip_ref,
    gain_ref,
    out_ref,
    next_x_ref,
    next_b_ref,
    next_c_ref,
    now_ref,
    rows_x_ref,
    rows_b_ref,
    rows_c_ref,
    sems,
):
    count, kept, channels = past_x_ref.shape
    tokens = step_ref.shape[0]
    steps = tokens // count
    heads = bias_ref.shape[1]
    states = short_ref.shape[2]
    groups = past_b_ref.shape[2] // states
    span = channels // groups
    starts = (0, channels, 2 * channels, 2 * channels + groups * states)

    for block in range(inner):
        for kind in range(4):
            low = sum(spans[:kind])
            total = None
            for shard in range(outer):
                term = parts_ref[shard * inner + block, :, low : low + spans[kind]].astype(
                    jnp.float32
                )
                total = term if total is None else total + term
            first = starts[kind] + block * spans[kind]
            now_ref[:, first : first + spans[kind]] = total.astype(jnp.bfloat16)

    stride = kept + 1

    def pick(rows, source_of, columns):
        row = lax.broadcasted_iota(jnp.int32, (rows, columns), 0)
        column = lax.broadcasted_iota(jnp.int32, (rows, columns), 1)
        return source_of(row, column)

    def from_past(row, column):
        found = jnp.zeros(row.shape, jnp.bool_)
        for s in range(count):
            place, seq = window_place(row)
            hit = (seq == s) & (place < CONV_W - 1)
            found = found | (hit & (column == s * stride + taken_ref[s] + place))
        return jnp.where(found, 1.0, 0.0).astype(jnp.bfloat16)

    def from_now(row, column):
        place, seq = window_place(row)
        hit = (place >= CONV_W - 1) & (place < kept)
        hit = hit & (column == seq * steps + place - (CONV_W - 1))
        return jnp.where(hit, 1.0, 0.0).astype(jnp.bfloat16)

    def window_place(row):
        tap, token = row // tokens, row % tokens
        other = row - CONV_W * tokens
        is_tap = row < CONV_W * tokens
        place = jnp.where(is_tap, tap + token % steps, other // count)
        seq = jnp.where(is_tap, token // steps, other % count)
        return place, seq

    rows = CONV_W * tokens + count * kept
    pick_past = pick(rows, from_past, count * stride)
    pick_now = pick(rows, from_now, tokens)

    moves = []

    def window(past_ref, first, taps_ref, next_ref, rows_ref):
        size = past_ref.shape[2]
        past = jnp.concatenate(
            [
                jnp.concatenate(
                    [past_ref[s].astype(jnp.float32), jnp.zeros((1, size), jnp.float32)], axis=0
                )
                for s in range(count)
            ],
            axis=0,
        ).astype(jnp.bfloat16)
        picked = jnp.dot(pick_past, past, preferred_element_type=jnp.float32) + jnp.dot(
            pick_now, now_ref[:, first : first + size], preferred_element_type=jnp.float32
        )
        for row in range(kept):
            low = CONV_W * tokens + row * count
            rows_ref[row] = picked[low : low + count].astype(jnp.bfloat16)
        moves.append(pltpu.make_async_copy(rows_ref, next_ref, sems.at[len(moves)]))
        moves[-1].start()
        return silu(
            sum(
                taps_ref[k : k + 1] * picked[k * tokens : (k + 1) * tokens] for k in range(CONV_W)
            )
        )

    x = window(past_x_ref, starts[1], conv_x_ref, next_x_ref, rows_x_ref)
    b = window(past_b_ref, starts[2], conv_b_ref, next_b_ref, rows_b_ref)
    c = window(past_c_ref, starts[3], conv_c_ref, next_c_ref, rows_c_ref)

    copies = spread(heads, channels // heads)
    fixed = jnp.dot(
        jnp.concatenate([bias_ref[...], decay_ref[...], skip_ref[...]], axis=0),
        copies,
        precision=lax.Precision.HIGHEST,
        preferred_element_type=jnp.float32,
    )
    dt = softplus(
        jnp.dot(step_ref[...], copies.astype(jnp.bfloat16), preferred_element_type=jnp.float32)
        + fixed[0:1]
    )
    one = -jnp.exp(fixed[1:2]) * dt
    place = lax.broadcasted_iota(jnp.int32, (tokens, 1), 0) % steps
    seq = lax.broadcasted_iota(jnp.int32, (tokens, 1), 0) // steps
    logs = one
    for back in range(1, steps):
        logs = logs + jnp.where(place >= back, pltpu.roll(one, back, 0), 0.0)

    c_short = c.astype(jnp.bfloat16)
    carried = []
    for group in range(groups):
        total = None
        for s in range(count):
            term = lax.dot_general(
                c_short[:, group * states : (group + 1) * states],
                short_ref[s, group * span : (group + 1) * span],
                (((1,), (1,)), ((), ())),
                preferred_element_type=jnp.float32,
            )
            total = term if total is None else jnp.where(seq == s, term, total)
        carried.append(total)
    y = jnp.exp(logs) * jnp.concatenate(carried, axis=1) + fixed[2:3] * x
    for back in range(steps):
        other_b = pltpu.roll(b, back, 0) if back else b
        score = jnp.concatenate(
            [
                jnp.broadcast_to(
                    jnp.sum(
                        (c * other_b)[:, g * states : (g + 1) * states], axis=1, keepdims=True
                    ),
                    (tokens, span),
                )
                for g in range(groups)
            ],
            axis=1,
        )
        if back:
            drop = jnp.where(place >= back, logs - pltpu.roll(logs, back, 0), 0.0)
            term = jnp.exp(drop) * score * pltpu.roll(dt * x, back, 0)
            y = y + jnp.where(place >= back, term, 0.0)
        else:
            y = y + score * (dt * x)
    g = y * silu(now_ref[:, 0:channels].astype(jnp.float32))
    for group in range(groups):
        cols = slice(group * span, (group + 1) * span)
        part = g[:, cols]
        mean = jnp.sum(part * part, axis=1, keepdims=True) * (1.0 / span)
        out_ref[:, cols] = (part * lax.rsqrt(mean + EPSILON) * gain_ref[:, cols]).astype(
            jnp.bfloat16
        )
    for move in moves:
        move.wait()


def make_mixer(outer, inner, spans, taken, parts, short, step, pasts, convs, vectors):
    tokens = step.shape[0]
    args = (close(parts), short, step) + pasts + convs + tuple(item[None] for item in vectors)
    channels = pasts[0].shape[2]
    vmem = pl.BlockSpec(memory_space=pltpu.VMEM)
    return pl.pallas_call(
        functools.partial(mixer_kernel, outer, inner, spans),
        in_specs=[pl.BlockSpec(memory_space=pltpu.SMEM)] + [vmem] * len(args),
        out_specs=[vmem] + [pl.BlockSpec(memory_space=pltpu.HBM)] * 3,
        out_shape=[pltpu.VMEM((tokens, channels), jnp.bfloat16)]
        + [jax.ShapeDtypeStruct(turned(item), jnp.bfloat16) for item in pasts],
        scratch_shapes=[
            pltpu.VMEM((tokens, sum(item.shape[2] for item in pasts) + channels), jnp.bfloat16)
        ]
        + [pltpu.VMEM(turned(item), jnp.bfloat16) for item in pasts]
        + [pltpu.SemaphoreType.DMA((3,))],
        cost_estimate=pl.CostEstimate(
            flops=4 * short.size * tokens, bytes_accessed=2 * short.size, transcendentals=0
        ),
        compiler_params=grant(12),
        name="mixer",
    )(taken, *args)


def product_kernel(outer, inner, *refs):
    ys, columns, out_ref = refs[:outer], refs[outer : outer + inner], refs[outer + inner]
    stacked = jnp.concatenate([item[...] for item in ys], axis=0)
    size = columns[0].shape[1]
    for step in range(inner):
        result = jnp.dot(stacked, columns[step][...], preferred_element_type=jnp.float32)
        out_ref[:, step * size : (step + 1) * size] = result.astype(jnp.bfloat16)


def make_product(ys, columns):
    outer, inner = len(ys), len(columns)
    tokens, depth = ys[0].shape
    size = columns[0].shape[1]
    vmem = pl.BlockSpec(memory_space=pltpu.VMEM)
    return pl.pallas_call(
        functools.partial(product_kernel, outer, inner),
        in_specs=[vmem] * (outer + inner),
        out_specs=vmem,
        out_shape=pltpu.VMEM((outer * tokens, inner * size), jnp.bfloat16),
        cost_estimate=pl.CostEstimate(
            flops=2 * outer * tokens * depth * inner * size,
            bytes_accessed=2 * depth * inner * size,
            transcendentals=0,
        ),
        compiler_params=grant(6),
        name="product",
    )(*[close(item) for item in (*ys, *columns)])


def join_kernel(left_ref, right_ref, *outs):
    tokens = outs[0].shape[0]
    for shard, out in enumerate(outs):
        rows = slice(shard * tokens, (shard + 1) * tokens)
        total = left_ref[rows].astype(jnp.float32) + right_ref[rows].astype(jnp.float32)
        out[...] = total.astype(jnp.bfloat16)


def make_joined(left, right, outer):
    tokens, columns = left.shape
    vmem = pl.BlockSpec(memory_space=pltpu.VMEM)
    return pl.pallas_call(
        join_kernel,
        in_specs=[vmem] * 2,
        out_specs=[vmem] * outer,
        out_shape=[pltpu.VMEM((tokens // outer, columns), jnp.bfloat16)] * outer,
        compiler_params=grant(2),
        name="join",
    )(close(left), close(right))


def arrange_kernel(outer, inner, *refs):
    out_ref = refs[outer]
    count, steps, _ = out_ref.shape
    size = refs[0].shape[1] // inner
    half = outer // 2
    me, side = lax.axis_index("kv"), lax.axis_index("tp")
    me_outer, me_inner = lax.div(me, inner), lax.rem(me, inner)
    for step in range(outer):
        shard = me_outer ^ step

        @pl.when(lax.div(shard, half) == side)
        def _(step=step, shard=shard):
            item = refs[step][...].astype(jnp.float32)
            for sub in range(inner):
                column = (lax.rem(shard, half) * inner + (me_inner ^ sub)) * size
                column = pl.multiple_of(column, size)
                for s in range(count):
                    block = item[s * steps : (s + 1) * steps, sub * size : (sub + 1) * size]
                    out_ref[s, :, pl.ds(column, size)] = block.astype(jnp.bfloat16)


def make_arranged(items, inner, count):
    outer = len(items)
    tokens, columns = items[0].shape
    vmem = pl.BlockSpec(memory_space=pltpu.VMEM)
    return pl.pallas_call(
        functools.partial(arrange_kernel, outer, inner),
        in_specs=[vmem] * outer,
        out_specs=vmem,
        out_shape=jax.ShapeDtypeStruct(
            (count, tokens // count, outer // 2 * columns), jnp.bfloat16
        ),
        compiler_params=grant(2),
        name="arrange",
    )(*[close(item) for item in items])


def inner_size(ranks):
    size = 1
    while ranks % (2 * size) == 0 and 4 * size * size <= ranks:
        size = 2 * size
    return size


def swap(item, step):
    ranks = lax.axis_size("kv")
    return lax.ppermute(item, "kv", [(k, k ^ step) for k in range(ranks)])


def whole_step(
    tokens,
    input_gain,
    gate_weight,
    value_weight,
    write_weight,
    read_weight,
    step_weight,
    conv_value,
    conv_write,
    conv_read,
    step_bias,
    decay_log,
    skip_gain,
    output_gain,
    out_weight,
    base_state,
    past_value,
    past_write,
    past_read,
    past_step,
    accepted,
):
    ranks = lax.axis_size("kv")
    halves = lax.axis_size("tp")
    me = lax.axis_index("kv")
    side = lax.axis_index("tp")
    inner = inner_size(ranks)
    outer = ranks // inner
    me_inner = lax.rem(me, inner)
    me_outer = lax.div(me, inner)

    weights = (gate_weight, value_weight, write_weight, read_weight)
    spans = [item.shape[1] // inner for item in weights]

    def piece(step):
        target = me_inner ^ step
        return jnp.concatenate(
            [
                lax.dynamic_slice_in_dim(item, target * span, span, 1)
                for item, span in zip(weights, spans)
            ],
            axis=1,
        )

    if any(span % 128 for span in spans):
        packed = [piece(step) for step in range(inner)]
    else:
        packed = make_packed(weights, tuple(spans), inner)
    narrow = [packed[0]]
    for step in range(1, inner):
        narrow.append(swap(packed[step], step))

    whole = lax.all_gather(tokens, "tp", axis=2, tiled=True)
    seq_local, proposals, width = whole.shape
    rows = whole.astype(jnp.float32)
    normed = (
        rows * lax.rsqrt(jnp.mean(rows * rows, axis=-1, keepdims=True) + EPSILON) * input_gain
    ).astype(jnp.bfloat16)
    flat = normed.reshape(seq_local * proposals, width)
    token_count = flat.shape[0]
    head_count = step_bias.shape[0]
    own_step = lax.dynamic_slice_in_dim(step_weight, side * head_count, head_count, 1)
    step_now = jnp.dot(flat, own_step, preferred_element_type=jnp.float32).astype(jnp.bfloat16)

    part = width // (outer * halves)
    share = lax.dynamic_index_in_dim(
        flat.reshape(token_count, outer, halves, part), side, 2, keepdims=False
    )
    share = jnp.broadcast_to(
        jnp.swapaxes(share, 0, 1)[:, None], (outer, inner, token_count, part)
    ).reshape(ranks * token_count, part)
    everyone = lax.all_to_all(share, "kv", split_axis=0, concat_axis=0, tiled=True)
    everyone = lax.all_gather(everyone, "tp", axis=1, tiled=True)

    block = width // ranks
    if block % 128 or sum(spans) % 128:
        product = None
        for step in range(inner):
            term = jnp.dot(
                lax.dynamic_slice_in_dim(everyone, (me_inner ^ step) * block, block, 1),
                narrow[step],
                preferred_element_type=jnp.float32,
            )
            product = term if product is None else product + term
        product = product.astype(jnp.bfloat16)
    else:
        product = make_partial(everyone, narrow)
    returned = lax.all_to_all(product, "kv", split_axis=0, concat_axis=0, tiled=True)
    columns = [out_weight]
    for step in range(1, inner):
        columns.append(swap(out_weight, step))
    returned = returned.reshape(ranks, token_count, sum(spans))
    shards, pieces = outer, inner
    if any(span % 128 for span in spans):
        summed = jnp.sum(
            returned.reshape(outer, inner, token_count, sum(spans)).astype(jnp.float32), axis=0
        ).astype(jnp.bfloat16)
        joined, offset = [], 0
        for span in spans:
            item = jnp.swapaxes(summed[:, :, offset : offset + span], 0, 1)
            joined.append(item.reshape(token_count, inner * span))
            offset = offset + span
        returned = jnp.concatenate(joined, axis=1)[None]
        spans = [inner * span for span in spans]
        shards, pieces = 1, 1

    root_state, short = make_root(
        base_state,
        past_value,
        past_write,
        past_step,
        accepted,
        conv_value,
        conv_write,
        step_bias,
        decay_log,
    )
    flat_y, *nexts = make_mixer(
        shards,
        pieces,
        tuple(spans),
        accepted,
        returned,
        short,
        step_now,
        (past_value, past_write, past_read),
        (conv_value, conv_write, conv_read),
        (step_bias, decay_log, skip_gain, output_gain),
    )
    next_value, next_write, next_read = [jnp.swapaxes(item, 0, 1) for item in nexts]
    ys = [flat_y] + [swap(flat_y, inner * step) for step in range(1, outer)]
    step_out = step_now.reshape(seq_local, proposals, head_count)
    if out_weight.shape[1] % 128 == 0 and halves == 2 and outer % 2 == 0:
        partial = make_product(ys, columns)
        keeper = [(k // inner) // (outer // 2) for k in range(ranks)]
        other = lax.ppermute(
            partial, ("kv", "tp"), [(2 * k + 1 - keeper[k], 2 * k + keeper[k]) for k in range(ranks)]
        )
        sums = make_joined(partial, other, outer)
        blocks = [sums[0]] + [
            lax.ppermute(
                sums[step],
                ("kv", "tp"),
                [(2 * k + keeper[k], 2 * (k ^ (inner * step)) + keeper[k]) for k in range(ranks)],
            )
            for step in range(1, outer)
        ]
        mixed = make_arranged(blocks, inner, seq_local)
        return (mixed, root_state, next_value, next_write, next_read, step_out)
    stacked = jnp.concatenate(ys, axis=0)
    partial = jnp.concatenate(
        [
            jnp.dot(stacked, item, preferred_element_type=jnp.float32).astype(jnp.bfloat16)
            for item in columns
        ],
        axis=1,
    ).reshape(outer, token_count, -1)
    blocks = jnp.stack(
        [partial[0]] + [swap(partial[step], inner * step) for step in range(1, outer)]
    ).reshape(outer, token_count, inner, -1)
    order_outer = me_outer ^ jnp.arange(outer)
    order_inner = me_inner ^ jnp.arange(inner)
    blocks = jnp.take(jnp.take(blocks, order_outer, axis=0), order_inner, axis=2)
    full = jnp.swapaxes(blocks, 0, 1).reshape(token_count, halves, width // halves)
    shares = lax.all_to_all(full, "tp", split_axis=1, concat_axis=1, tiled=True)
    mixed = jnp.sum(shares.astype(jnp.float32), axis=1).astype(jnp.bfloat16)
    mixed = mixed.reshape(seq_local, proposals, width // halves)
    return (mixed, root_state, next_value, next_write, next_read, step_out)


def solution(mesh):
    return jax.shard_map(
        whole_step,
        mesh=mesh,
        in_specs=(
            P("kv", None, "tp"),
            P(),
            P("kv", "tp"),
            P("kv", "tp"),
            P("kv", "tp"),
            P("kv", "tp"),
            P(),
            P(None, "tp"),
            P(None, "tp"),
            P(None, "tp"),
            P("tp"),
            P("tp"),
            P("tp"),
            P("tp"),
            P("tp", "kv"),
            P("kv", "tp", None, None),
            P("kv", None, "tp"),
            P("kv", None, "tp"),
            P("kv", None, "tp"),
            P("kv", None, "tp"),
            P("kv"),
        ),
        out_specs=(
            P("kv", None, "tp"),
            P("kv", "tp", None, None),
            P("kv", None, "tp"),
            P("kv", None, "tp"),
            P("kv", None, "tp"),
            P("kv", None, "tp"),
        ),
        check_vma=False,
    )
```

profile of v0, /device:TPU:0, one launch (start us, length us, event | category | flops | bytes accessed | tf_op | source)
XLA Modules:
  0.0 79.3 jit_solution(3946183104144156856)
XLA Ops:
  0.6 0.0 copy-start
  0.7 1.6 %pack.1 = (bf16[128,1280]{1,0:T(8,128)(2,1)S(1)}, bf16[128,1280]{1,0:T(8,128)(2,1)S(1)}, bf16[128,1280]{1,0:T(8,128)(2,1)S(1)}, bf16[128,1280]{1,0:T(8,128)(2,1)S(1)}) custom-call(bf16[128,2048]{1,0:T(8,128)(2,1)} %gate_ref.1, bf16[128,2048]{1,0:T(8,128)(2,1)} %value_ref.1, bf16[128,512]{1,0:T(8,128)(2,1)} %write_ref.1, bf16[128,512]{1,0:T(8,128)(2,1)} %read_ref.1), custom_call_target="tpu_custom_call" | custom-call | tf_op jit(solution)/shard_map/pack/pallas_call | solution.py:71
  2.4 3.0 %collective-permute-start = (bf16[128,1280]{1,0:T(8,128)(2,1)S(1)}, bf16[128,1280]{1,0:T(8,128)(2,1)S(1)}, u32[]{:S(2)}, u32[]{:S(2)}) collective-permute-start(bf16[128,1280]{1,0:T(8,128)(2,1)S(1)} %get-tuple-element.21), channel_id=1, source_target_pairs={{0,2},{2,0},{4,6},{6,4},{8,10},{10,8},{12,14},{14,12},{16,18},{18,... | collective-permute-start | bytes 983048 | tf_op jit(solution)/shard_map/ppermute | solution.py:511
  5.4 1.5 %collective-permute-start.1 = (bf16[128,1280]{1,0:T(8,128)(2,1)S(1)}, bf16[128,1280]{1,0:T(8,128)(2,1)S(1)}, u32[]{:S(2)}, u32[]{:S(2)}) collective-permute-start(bf16[128,1280]{1,0:T(8,128)(2,1)S(1)} %get-tuple-element.22), channel_id=1, source_target_pairs={{0,4},{2,6},{4,0},{6,2},{8,12},{10,14},{12,8},{14,10},{16,20},{18,... | collective-permute-start | bytes 983048 | tf_op jit(solution)/shard_map/ppermute | solution.py:511
  6.9 0.0 collective-permute-start.2
  6.9 2.1 %all_gather.6 = bf16[4,4,2048]{2,1,0:T(4,128)(2,1)S(1)} all-gather(bf16[4,4,1024]{2,1,0:T(4,128)(2,1)} %param.21), channel_id=1, replica_groups=mesh['kv'=16,'tp'=2] {'tp'}, dimensions={2}, use_global_device_ids=true | all-gather | bytes 98304 | tf_op jit(solution)/shard_map/all_gather | solution.py:567
  9.0 0.1 fusion
  9.1 0.8 %fusion.2 = bf16[4,4,2048]{2,1,0:T(4,128)(2,1)S(1)} fusion(bf16[4,4,2048]{2,1,0:T(4,128)(2,1)S(1)} %all_gather.6, f32[2048]{0:T(1024)} %param.22, f32[4,4]{1,0:T(4,128)S(1)} %add_rsqrt_fusion), kind=kLoop, calls=%fused_computation.5 | loop fusion | flops 131072 | bytes 139328 | tf_op jit(solution)/shard_map/convert_element_type | solution.py:572
  10.0 0.1 constant_dynamic-slice_fusion
  10.1 14.9 %all_to_all.21 = bf16[16,16,256]{2,1,0:T(8,128)(2,1)S(1)} all-to-all(bf16[16,16,256]{2,1,0:T(8,128)(2,1)S(1)} %bitcast.25), channel_id=1, replica_groups=mesh['kv'=16,'tp'=2] {'kv'}, dimensions={0} | all-to-all | bytes 262144 | tf_op jit(solution)/shard_map/all_to_all | solution.py:586
  25.0 2.0 %all_gather.7.rows_ref = bf16[256,512]{1,0:T(8,128)(2,1)S(1)} all-gather(bf16[256,256]{1,0:T(8,128)(2,1)S(1)} %bitcast.24), channel_id=1, replica_groups=mesh['kv'=16,'tp'=2] {'tp'}, dimensions={1}, use_global_device_ids=true | all-gather | bytes 393216 | tf_op jit(solution)/shard_map/all_gather | solution.py:587
  27.0 0.0 collective-permute-done.refs_1_
  27.0 0.0 collective-permute-done.1.refs_2_
  27.0 0.0 collective-permute-done.2.refs_3_
  27.0 0.0 copy-start.5
  27.0 0.0 copy-start.6
  27.0 0.0 copy-start.11
  27.1 1.7 %partial.1 = bf16[256,1280]{1,0:T(8,128)(2,1)} custom-call(bf16[256,512]{1,0:T(8,128)(2,1)S(1)} %all_gather.7.rows_ref, bf16[128,1280]{1,0:T(8,128)(2,1)S(1)} %get-tuple-element.20.refs_0_, bf16[128,1280]{1,0:T(8,128)(2,1)S(1)} %collective-permute-done.refs_1_, bf16[128,1280]{1,0:T(8,128)(2,1)S(1)} %collective-permute-done.1.refs_2_, ...), custom_call_target="tpu_custom_call" | custom-call | flops 335544320 | bytes 655360 | tf_op jit(solution)/shard_map/partial/pallas_call | solution.py:101
  28.7 3.9 %all-to-all-start.1 = ((bf16[16,16,1280]{2,1,0:T(8,128)(2,1)}), bf16[16,16,1280]{2,1,0:T(8,128)(2,1)S(1)}, u32[]{:S(2)}, u32[]{:S(2)}) async-start(bf16[16,16,1280]{2,1,0:T(8,128)(2,1)} %bitcast.4), calls=%async_computation.1 | async-start | bytes 1310720 | tf_op jit(solution)/shard_map/all_to_all | solution.py:602
  32.6 1.9 %collective-permute-start.6 = (bf16[2048,128]{1,0:T(8,128)(2,1)}, bf16[2048,128]{1,0:T(8,128)(2,1)}, u32[]{:S(2)}, u32[]{:S(2)}) collective-permute-start(bf16[2048,128]{1,0:T(8,128)(2,1)} %refs_4_.1), channel_id=1, source_target_pairs={{0,2},{2,0},{4,6},{6,4},{8,10},{10,8},{12,14},{14,12},{16,18},{18,... | collective-permute-start | bytes 1572872 | tf_op jit(solution)/shard_map/ppermute | solution.py:511
  34.6 1.5 %collective-permute-start.7 = (bf16[2048,128]{1,0:T(8,128)(2,1)}, bf16[2048,128]{1,0:T(8,128)(2,1)}, u32[]{:S(2)}, u32[]{:S(2)}) collective-permute-start(bf16[2048,128]{1,0:T(8,128)(2,1)} %refs_4_.1), channel_id=1, source_target_pairs={{0,4},{2,6},{4,0},{6,2},{8,12},{10,14},{12,8},{14,10},{16,20},{18,... | collective-permute-start | bytes 1572872 | tf_op jit(solution)/shard_map/ppermute | solution.py:511
  36.0 0.2 collective-permute-start.8
  36.2 0.1 copy.38.past_x_ref
  36.4 0.0 copy-start.1
  36.4 2.2 %copy-done.1 = f32[4,32,64,128]{3,2,1,0:T(8,128)S(1)} copy-done((f32[4,32,64,128]{3,2,1,0:T(8,128)S(1)}, f32[4,32,64,128]{3,2,1,0:T(8,128)}, u32[]{:S(2)}) %copy-start.1) | copy-done | bytes 4194328
  38.6 4.9 %root.1 = (f32[4,32,64,128]{3,2,1,0:T(8,128)}, bf16[4,2048,128]{2,1,0:T(8,128)(2,1)S(1)}) custom-call(s32[4]{0:T(128)S(1)} %copy-done.8, f32[4,32,64,128]{3,2,1,0:T(8,128)S(1)} %copy-done.1, bf16[4,7,2048]{2,1,0:T(8,128)(2,1)S(1)} %copy.38.past_x_ref, bf16[4,7,512]{2,1,0:T(8,128)(2,1)S(1)} %copy.39.past_b_ref, bf16[4,4,32]{2,1,0:T(4,128)(2,1)S(1)} %copy-done.7, ...), custom_call_target="tpu_custom_call" | custom-call | flops 67108864 | bytes 10485760 | tf_op jit(solution)/shard_map/root/pallas_call | solution.py:195
  43.5 0.1 convolution_convert_fusion.step_ref
  43.6 6.7 %all-to-all-done.1.parts_ref = bf16[16,16,1280]{2,1,0:T(8,128)(2,1)S(1)} async-done(((bf16[16,16,1280]{2,1,0:T(8,128)(2,1)}), bf16[16,16,1280]{2,1,0:T(8,128)(2,1)S(1)}, u32[]{:S(2)}, u32[]{:S(2)}) %all-to-all-start.1) | async-done | bytes 655392 | tf_op jit(solution)/shard_map/all_to_all | solution.py:602
  50.3 2.3 %mixer.1 = (bf16[16,2048]{1,0:T(8,128)(2,1)S(1)}, bf16[7,4,2048]{2,1,0:T(4,128)(2,1)}, bf16[7,4,512]{2,1,0:T(4,128)(2,1)}, bf16[7,4,512]{2,1,0:T(4,128)(2,1)}) custom-call(s32[4]{0:T(128)S(1)} %copy-done.8, bf16[16,16,1280]{2,1,0:T(8,128)(2,1)S(1)} %all-to-all-done.1.parts_ref, bf16[4,2048,128]{2,1,0:T(8,128)(2,1)S(1)} %get-tuple-element.24.short_ref, ...), custom_call_target="tpu_custom_call" | custom-call | flops 67108864 | bytes 2097152 | tf_op jit(solution)/shard_map/mixer/pallas_call | solution.py:396
  52.7 1.9 %collective-permute-start.3 = (bf16[16,2048]{1,0:T(8,128)(2,1)S(1)}, bf16[16,2048]{1,0:T(8,128)(2,1)S(1)}, u32[]{:S(2)}, u32[]{:S(2)}) collective-permute-start(bf16[16,2048]{1,0:T(8,128)(2,1)S(1)} %get-tuple-element.25.refs_0_), channel_id=1, source_target_pairs={{0,8},{2,10},{4,12},{6,14},{8,0},{10,2},{12,4},{14,6},{16,24},{18,... | collective-permute-start | bytes 196616 | tf_op jit(solution)/shard_map/ppermute | solution.py:511
  54.6 0.7 collective-permute-start.4
  55.3 0.0 collective-permute-done.6.refs_5_
  55.3 2.5 %collective-permute-start.5 = (bf16[16,2048]{1,0:T(8,128)(2,1)S(1)}, bf16[16,2048]{1,0:T(8,128)(2,1)S(1)}, u32[]{:S(2)}, u32[]{:S(2)}) collective-permute-start(bf16[16,2048]{1,0:T(8,128)(2,1)S(1)} %get-tuple-element.25.refs_0_), channel_id=1, source_target_pairs={{0,24},{2,26},{4,28},{6,30},{8,16},{10,18},{12,20},{14,22},{16,8},... | collective-permute-start | bytes 196616 | tf_op jit(solution)/shard_map/ppermute | solution.py:511
  57.8 0.0 collective-permute-done.7.refs_6_
  57.8 7.9 %collective-permute-done.8.refs_7_ = bf16[2048,128]{1,0:T(8,128)(2,1)} collective-permute-done((bf16[2048,128]{1,0:T(8,128)(2,1)}, bf16[2048,128]{1,0:T(8,128)(2,1)}, u32[]{:S(2)}, u32[]{:S(2)}) %collective-permute-start.8) | collective-permute-done | bytes 524320 | tf_op jit(solution)/shard_map/ppermute | solution.py:511
  65.7 0.0 collective-permute-done.3.refs_1_
  65.7 0.0 collective-permute-done.4.refs_2_
  65.7 0.0 collective-permute-done.5.refs_3_
  65.7 2.0 %product.1.left_ref = bf16[64,512]{1,0:T(8,128)(2,1)S(1)} custom-call(bf16[16,2048]{1,0:T(8,128)(2,1)S(1)} %get-tuple-element.25.refs_0_, bf16[16,2048]{1,0:T(8,128)(2,1)S(1)} %collective-permute-done.3.refs_1_, bf16[16,2048]{1,0:T(8,128)(2,1)S(1)} %collective-permute-done.4.refs_2_, bf16[16,2048]{1,0:T(8,128)(2,1)S(1)} %collective-permute-done.5.refs_3_, ...), custom_call_target="tpu_custom_call" | custom-call | flops 134217728 | bytes 2097152 | tf_op jit(solution)/shard_map/product/pallas_call | solution.py:429
  67.7 1.3 %collective-permute-start.9 = (bf16[64,512]{1,0:T(8,128)(2,1)S(1)}, bf16[64,512]{1,0:T(8,128)(2,1)S(1)}, u32[]{:S(2)}, u32[]{:S(2)}) collective-permute-start(bf16[64,512]{1,0:T(8,128)(2,1)S(1)} %product.1.left_ref), channel_id=1, source_target_pairs={{1,0},{3,2},{5,4},{7,6},{9,8},{11,10},{13,12},{15,14},{16,17},{18,... | collective-permute-start | bytes 196616 | tf_op jit(solution)/shard_map/ppermute | solution.py:650
  69.0 1.8 %collective-permute-done.9.right_ref = bf16[64,512]{1,0:T(8,128)(2,1)S(1)} collective-permute-done((bf16[64,512]{1,0:T(8,128)(2,1)S(1)}, bf16[64,512]{1,0:T(8,128)(2,1)S(1)}, u32[]{:S(2)}, u32[]{:S(2)}) %collective-permute-start.9) | collective-permute-done | bytes 65568 | tf_op jit(solution)/shard_map/ppermute | solution.py:650
  70.8 3.4 %collective-permute-start.10 = (bf16[16,512]{1,0:T(8,128)(2,1)S(1)}, bf16[16,512]{1,0:T(8,128)(2,1)S(1)}, u32[]{:S(2)}, u32[]{:S(2)}) collective-permute-start(bf16[16,512]{1,0:T(8,128)(2,1)S(1)} %get-tuple-element.27), channel_id=1, source_target_pairs={{0,8},{2,10},{4,12},{6,14},{8,0},{10,2},{12,4},{14,6},{17,25},{19,... | collective-permute-start | bytes 49160 | tf_op jit(solution)/shard_map/ppermute | solution.py:655
  74.2 1.3 %collective-permute-start.11 = (bf16[16,512]{1,0:T(8,128)(2,1)S(1)}, bf16[16,512]{1,0:T(8,128)(2,1)S(1)}, u32[]{:S(2)}, u32[]{:S(2)}) collective-permute-start(bf16[16,512]{1,0:T(8,128)(2,1)S(1)} %get-tuple-element.28), channel_id=1, source_target_pairs={{0,16},{2,18},{4,20},{6,22},{8,24},{10,26},{12,28},{14,30},{17,1},... | collective-permute-start | bytes 49160 | tf_op jit(solution)/shard_map/ppermute | solution.py:655
  75.5 1.7 %collective-permute-start.12 = (bf16[16,512]{1,0:T(8,128)(2,1)S(1)}, bf16[16,512]{1,0:T(8,128)(2,1)S(1)}, u32[]{:S(2)}, u32[]{:S(2)}) collective-permute-start(bf16[16,512]{1,0:T(8,128)(2,1)S(1)} %get-tuple-element.29), channel_id=1, source_target_pairs={{0,24},{2,26},{4,28},{6,30},{8,16},{10,18},{12,20},{14,22},{17,9},... | collective-permute-start | bytes 49160 | tf_op jit(solution)/shard_map/ppermute | solution.py:655
  77.2 0.0 collective-permute-done.10.refs_1_
  77.2 0.0 collective-permute-done.11.refs_2_
  77.2 1.4 %collective-permute-done.12.refs_3_ = bf16[16,512]{1,0:T(8,128)(2,1)S(1)} collective-permute-done((bf16[16,512]{1,0:T(8,128)(2,1)S(1)}, bf16[16,512]{1,0:T(8,128)(2,1)S(1)}, u32[]{:S(2)}, u32[]{:S(2)}) %collective-permute-start.12) | collective-permute-done | bytes 16416 | tf_op jit(solution)/shard_map/ppermute | solution.py:655
  78.6 0.7 arrange.1
  (32 shorter events, 0.2 us)
Async XLA Ops:
  0.6 42.8 %copy-start = (bf16[2048,64]{0,1:T(8,128)(2,1)S(1)}, bf16[2048,64]{0,1:T(8,128)(2,1)}, u32[]{:S(2)}) copy-start(bf16[2048,64]{0,1:T(8,128)(2,1)} %param.27) | copy-start | bytes 786436
  0.7 35.6 %copy-start.12 = (bf16[4,7,2048]{2,0,1:T(4,128)(2,1)S(1)}, bf16[4,7,2048]{2,0,1:T(4,128)(2,1)}, u32[]{:S(2)}) copy-start(bf16[4,7,2048]{2,0,1:T(4,128)(2,1)} %param.37) | copy-start | bytes 344068
  0.7 35.6 %copy-start.13 = (bf16[4,7,512]{2,0,1:T(4,128)(2,1)S(1)}, bf16[4,7,512]{2,0,1:T(4,128)(2,1)}, u32[]{:S(2)}) copy-start(bf16[4,7,512]{2,0,1:T(4,128)(2,1)} %param.38) | copy-start | bytes 86020
  0.7 35.6 %copy-start.14 = (bf16[4,7,512]{2,0,1:T(4,128)(2,1)S(1)}, bf16[4,7,512]{2,0,1:T(4,128)(2,1)}, u32[]{:S(2)}) copy-start(bf16[4,7,512]{2,0,1:T(4,128)(2,1)} %param.39) | copy-start | bytes 86020
  0.7 35.7 %copy-start.9 = (f32[32]{0:T(128)S(1)}, f32[32]{0:T(128)}, u32[]{:S(2)}) copy-start(f32[32]{0:T(128)} %param.31) | copy-start | bytes 388
  0.7 35.7 %copy-start.10 = (f32[32]{0:T(128)S(1)}, f32[32]{0:T(128)}, u32[]{:S(2)}) copy-start(f32[32]{0:T(128)} %param.32) | copy-start | bytes 388
  0.7 35.7 %copy-start.2 = (f32[4,2048]{1,0:T(4,128)S(1)}, f32[4,2048]{1,0:T(4,128)}, u32[]{:S(2)}) copy-start(f32[4,2048]{1,0:T(4,128)} %conv_x_ref.3) | copy-start | bytes 98308
  0.7 35.7 %copy-start.3 = (f32[4,512]{1,0:T(4,128)S(1)}, f32[4,512]{1,0:T(4,128)}, u32[]{:S(2)}) copy-start(f32[4,512]{1,0:T(4,128)} %conv_b_ref.3) | copy-start | bytes 24580
  0.7 35.7 %copy-start.7 = (bf16[4,4,32]{2,1,0:T(4,128)(2,1)S(1)}, bf16[4,4,32]{2,1,0:T(4,128)(2,1)}, u32[]{:S(2)}) copy-start(bf16[4,4,32]{2,1,0:T(4,128)(2,1)} %past_dt_ref.1) | copy-start | bytes 3076
  0.7 35.7 %copy-start.8 = (s32[4]{0:T(128)S(1)}, s32[4]{0:T(128)}, u32[]{:S(2)}) copy-start(s32[4]{0:T(128)} %taken_ref.3) | copy-start | bytes 52
  2.4 24.6 %collective-permute-start = (bf16[128,1280]{1,0:T(8,128)(2,1)S(1)}, bf16[128,1280]{1,0:T(8,128)(2,1)S(1)}, u32[]{:S(2)}, u32[]{:S(2)}) collective-permute-start(bf16[128,1280]{1,0:T(8,128)(2,1)S(1)} %get-tuple-element.21), channel_id=1, source_target_pairs={{0,2},{2,0},{4,6},{6,4},{8,10},{10,8},{12,14},{14,12},{16,18},{18,... | collective-permute-start | bytes 983048 | tf_op jit(solution)/shard_map/ppermute | solution.py:511
  5.4 21.6 %collective-permute-start.1 = (bf16[128,1280]{1,0:T(8,128)(2,1)S(1)}, bf16[128,1280]{1,0:T(8,128)(2,1)S(1)}, u32[]{:S(2)}, u32[]{:S(2)}) collective-permute-start(bf16[128,1280]{1,0:T(8,128)(2,1)S(1)} %get-tuple-element.22), channel_id=1, source_target_pairs={{0,4},{2,6},{4,0},{6,2},{8,12},{10,14},{12,8},{14,10},{16,20},{18,... | collective-permute-start | bytes 983048 | tf_op jit(solution)/shard_map/ppermute | solution.py:511
  6.9 20.1 %collective-permute-start.2 = (bf16[128,1280]{1,0:T(8,128)(2,1)S(1)}, bf16[128,1280]{1,0:T(8,128)(2,1)S(1)}, u32[]{:S(2)}, u32[]{:S(2)}) collective-permute-start(bf16[128,1280]{1,0:T(8,128)(2,1)S(1)} %get-tuple-element.23), channel_id=1, source_target_pairs={{0,6},{2,4},{4,2},{6,0},{8,14},{10,12},{12,10},{14,8},{16,22},{18,... | collective-permute-start | bytes 983048 | tf_op jit(solution)/shard_map/ppermute | solution.py:511
  27.0 23.3 %copy-start.5 = (f32[4,512]{1,0:T(4,128)S(1)}, f32[4,512]{1,0:T(4,128)}, u32[]{:S(2)}) copy-start(f32[4,512]{1,0:T(4,128)} %conv_c_ref.1) | copy-start | bytes 24580
  27.0 23.3 %copy-start.6 = (f32[2048]{0:T(1024)S(1)}, f32[2048]{0:T(1024)}, u32[]{:S(2)}) copy-start(f32[2048]{0:T(1024)} %param.34) | copy-start | bytes 24580
  27.0 23.3 %copy-start.11 = (f32[32]{0:T(128)S(1)}, f32[32]{0:T(128)}, u32[]{:S(2)}) copy-start(f32[32]{0:T(128)} %param.33) | copy-start | bytes 388
  28.7 21.6 %all-to-all-start.1 = ((bf16[16,16,1280]{2,1,0:T(8,128)(2,1)}), bf16[16,16,1280]{2,1,0:T(8,128)(2,1)S(1)}, u32[]{:S(2)}, u32[]{:S(2)}) async-start(bf16[16,16,1280]{2,1,0:T(8,128)(2,1)} %bitcast.4), calls=%async_computation.1 | async-start | bytes 1310720 | tf_op jit(solution)/shard_map/all_to_all | solution.py:602
  32.6 22.6 %collective-permute-start.6 = (bf16[2048,128]{1,0:T(8,128)(2,1)}, bf16[2048,128]{1,0:T(8,128)(2,1)}, u32[]{:S(2)}, u32[]{:S(2)}) collective-permute-start(bf16[2048,128]{1,0:T(8,128)(2,1)} %refs_4_.1), channel_id=1, source_target_pairs={{0,2},{2,0},{4,6},{6,4},{8,10},{10,8},{12,14},{14,12},{16,18},{18,... | collective-permute-start | bytes 1572872 | tf_op jit(solution)/shard_map/ppermute | solution.py:511
  34.6 23.2 %collective-permute-start.7 = (bf16[2048,128]{1,0:T(8,128)(2,1)}, bf16[2048,128]{1,0:T(8,128)(2,1)}, u32[]{:S(2)}, u32[]{:S(2)}) collective-permute-start(bf16[2048,128]{1,0:T(8,128)(2,1)} %refs_4_.1), channel_id=1, source_target_pairs={{0,4},{2,6},{4,0},{6,2},{8,12},{10,14},{12,8},{14,10},{16,20},{18,... | collective-permute-start | bytes 1572872 | tf_op jit(solution)/shard_map/ppermute | solution.py:511
  36.0 29.7 %collective-permute-start.8 = (bf16[2048,128]{1,0:T(8,128)(2,1)}, bf16[2048,128]{1,0:T(8,128)(2,1)}, u32[]{:S(2)}, u32[]{:S(2)}) collective-permute-start(bf16[2048,128]{1,0:T(8,128)(2,1)} %refs_4_.1), channel_id=1, source_target_pairs={{0,6},{2,4},{4,2},{6,0},{8,14},{10,12},{12,10},{14,8},{16,22},{18,... | collective-permute-start | bytes 1572872 | tf_op jit(solution)/shard_map/ppermute | solution.py:511
  36.4 2.2 %copy-start.1 = (f32[4,32,64,128]{3,2,1,0:T(8,128)S(1)}, f32[4,32,64,128]{3,2,1,0:T(8,128)}, u32[]{:S(2)}) copy-start(f32[4,32,64,128]{3,2,1,0:T(8,128)} %base_ref.1) | copy-start | bytes 12582916
  43.6 35.7 %copy-start.4 = (bf16[16,32]{1,0:T(8,128)(2,1)}, bf16[16,32]{1,0:T(8,128)(2,1)S(1)}, u32[]{:S(2)}) copy-start(bf16[16,32]{1,0:T(8,128)(2,1)S(1)} %convolution_convert_fusion.step_ref) | copy-start | bytes 3076
  52.7 13.0 %collective-permute-start.3 = (bf16[16,2048]{1,0:T(8,128)(2,1)S(1)}, bf16[16,2048]{1,0:T(8,128)(2,1)S(1)}, u32[]{:S(2)}, u32[]{:S(2)}) collective-permute-start(bf16[16,2048]{1,0:T(8,128)(2,1)S(1)} %get-tuple-element.25.refs_0_), channel_id=1, source_target_pairs={{0,8},{2,10},{4,12},{6,14},{8,0},{10,2},{12,4},{14,6},{16,24},{18,... | collective-permute-start | bytes 196616 | tf_op jit(solution)/shard_map/ppermute | solution.py:511
  54.6 11.1 %collective-permute-start.4 = (bf16[16,2048]{1,0:T(8,128)(2,1)S(1)}, bf16[16,2048]{1,0:T(8,128)(2,1)S(1)}, u32[]{:S(2)}, u32[]{:S(2)}) collective-permute-start(bf16[16,2048]{1,0:T(8,128)(2,1)S(1)} %get-tuple-element.25.refs_0_), channel_id=1, source_target_pairs={{0,16},{2,18},{4,20},{6,22},{8,24},{10,26},{12,28},{14,30},{16,0},... | collective-permute-start | bytes 196616 | tf_op jit(solution)/shard_map/ppermute | solution.py:511
  55.3 10.4 %collective-permute-start.5 = (bf16[16,2048]{1,0:T(8,128)(2,1)S(1)}, bf16[16,2048]{1,0:T(8,128)(2,1)S(1)}, u32[]{:S(2)}, u32[]{:S(2)}) collective-permute-start(bf16[16,2048]{1,0:T(8,128)(2,1)S(1)} %get-tuple-element.25.refs_0_), channel_id=1, source_target_pairs={{0,24},{2,26},{4,28},{6,30},{8,16},{10,18},{12,20},{14,22},{16,8},... | collective-permute-start | bytes 196616 | tf_op jit(solution)/shard_map/ppermute | solution.py:511
  67.7 3.1 %collective-permute-start.9 = (bf16[64,512]{1,0:T(8,128)(2,1)S(1)}, bf16[64,512]{1,0:T(8,128)(2,1)S(1)}, u32[]{:S(2)}, u32[]{:S(2)}) collective-permute-start(bf16[64,512]{1,0:T(8,128)(2,1)S(1)} %product.1.left_ref), channel_id=1, source_target_pairs={{1,0},{3,2},{5,4},{7,6},{9,8},{11,10},{13,12},{15,14},{16,17},{18,... | collective-permute-start | bytes 196616 | tf_op jit(solution)/shard_map/ppermute | solution.py:650
  70.8 6.4 %collective-permute-start.10 = (bf16[16,512]{1,0:T(8,128)(2,1)S(1)}, bf16[16,512]{1,0:T(8,128)(2,1)S(1)}, u32[]{:S(2)}, u32[]{:S(2)}) collective-permute-start(bf16[16,512]{1,0:T(8,128)(2,1)S(1)} %get-tuple-element.27), channel_id=1, source_target_pairs={{0,8},{2,10},{4,12},{6,14},{8,0},{10,2},{12,4},{14,6},{17,25},{19,... | collective-permute-start | bytes 49160 | tf_op jit(solution)/shard_map/ppermute | solution.py:655
  74.2 3.0 %collective-permute-start.11 = (bf16[16,512]{1,0:T(8,128)(2,1)S(1)}, bf16[16,512]{1,0:T(8,128)(2,1)S(1)}, u32[]{:S(2)}, u32[]{:S(2)}) collective-permute-start(bf16[16,512]{1,0:T(8,128)(2,1)S(1)} %get-tuple-element.28), channel_id=1, source_target_pairs={{0,16},{2,18},{4,20},{6,22},{8,24},{10,26},{12,28},{14,30},{17,1},... | collective-permute-start | bytes 49160 | tf_op jit(solution)/shard_map/ppermute | solution.py:655
  75.5 3.1 %collective-permute-start.12 = (bf16[16,512]{1,0:T(8,128)(2,1)S(1)}, bf16[16,512]{1,0:T(8,128)(2,1)S(1)}, u32[]{:S(2)}, u32[]{:S(2)}) collective-permute-start(bf16[16,512]{1,0:T(8,128)(2,1)S(1)} %get-tuple-element.29), channel_id=1, source_target_pairs={{0,24},{2,26},{4,28},{6,30},{8,16},{10,18},{12,20},{14,22},{17,9},... | collective-permute-start | bytes 49160 | tf_op jit(solution)/shard_map/ppermute | solution.py:655
where the time goes:
time: 79.9 us; the launch traced here: 79.3 us
  starting transfers between devices  24.8 us (31%)
  blocking collectives  19 us (24%)
  waiting for transfers between devices  17.8 us (22%)
  Pallas kernels  13.1 us (16%)
  local copies, waits for them, and re-layouts  2.51 us (3%)
  between operations  0.98 us (1%)
  other arithmetic  0.94 us (1%)
    all_to_all x1, blocking collectives, whole_step(): lax.all_to_all(share, 'kv', split_axis=0, concat_axis=0, tiled=True)  14.9 us
    ppermute x9, starting transfers between devices, swap(): return lax.ppermute(item, 'kv', [(k, k ^ step) for k in range(ranks)])  13.2 us
    ppermute x9, waiting for transfers between devices, swap(): return lax.ppermute(item, 'kv', [(k, k ^ step) for k in range(ranks)])  7.92 us
    all_to_all x1, waiting for transfers between devices, whole_step(): lax.all_to_all(product, 'kv', split_axis=0, concat_axis=0, tiled=True)  6.67 us
    ppermute x3, starting transfers between devices, whole_step(): lax.ppermute(sums[step], ('kv', 'tp'), [(2 * k + keeper[k], 2 * (k ^ inne...  6.35 us
    pallas_call x1, Pallas kernels, make_root(): pl.pallas_call(root_kernel, grid=(count,), in_specs=[pl.BlockSpec(memory_...  4.89 us
    all_to_all x1, starting transfers between devices, whole_step(): lax.all_to_all(product, 'kv', split_axis=0, concat_axis=0, tiled=True)  3.91 us
    unnamed x33, local copies, waits for them, and re-layouts  2.35 us
  transfers between devices with their start and end apart: 14, of which 4 were waited for; matrix products, arithmetic and copies ran while one was open for 2% of the time, Pallas kernels for 9%

commit v1 on v0

--- a/solution.py
+++ b/solution.py
@@ -35,8 +35,8 @@
     return pltpu.CompilerParams(vmem_limit_bytes=mib * 1024 * 1024)
 
 
-def turned(item):
-    return (item.shape[1], item.shape[0]) + item.shape[2:]
+def apart(item):
+    return pltpu.with_memory_space_constraint(item, pltpu.HBM)
 
 
 def close(item):
@@ -111,6 +111,38 @@
     )(close(rows), *[close(item) for item in weights])
 
 
+def hold_kernel(from_ref, to_ref, sem):
+    copy = pltpu.make_async_copy(from_ref, to_ref, sem)
+    copy.start()
+    copy.wait()
+
+
+def make_held(item):
+    return pl.pallas_call(
+        hold_kernel,
+        in_specs=[pl.BlockSpec(memory_space=pltpu.HBM)],
+        out_specs=pl.BlockSpec(memory_space=pltpu.VMEM),
+        out_shape=pltpu.VMEM(item.shape, item.dtype),
+        scratch_shapes=[pltpu.SemaphoreType.DMA],
+        cost_estimate=pl.CostEstimate(
+            flops=item.size * 64, bytes_accessed=4 * item.size, transcendentals=0
+        ),
+        compiler_params=grant(2),
+        name="hold",
+    )(apart(item))
+
+
+def place_in(rows, cols, source):
+    row = lax.broadcasted_iota(jnp.int32, (rows, cols), 0)
+    column = lax.broadcasted_iota(jnp.int32, (rows, cols), 1)
+    return jnp.where(column == source(row), 1.0, 0.0).astype(jnp.bfloat16)
+
+
+def stacked_rows(ref):
+    rows = [ref[k].astype(jnp.float32) for k in range(ref.shape[0])]
+    return jnp.concatenate(rows, axis=0).astype(jnp.bfloat16)
+
+
 def root_kernel(
     taken_ref,
     base_ref,
@@ -121,53 +153,100 @@
     conv_b_ref,
     bias_ref,
     decay_ref,
+    rows_ref,
+    step_weight_ref,
     root_ref,
     short_ref,
+    step_ref,
+    step_out_ref,
+    lhs_ref,
+    rhs_ref,
 ):
     _, heads, width, states = base_ref.shape
-    steps = past_dt_ref.shape[1]
+    count, steps = past_dt_ref.shape[:2]
+    tokens = count * steps
     groups = past_b_ref.shape[2] // states
     span = heads * width // groups
-    taken = taken_ref[pl.program_id(0)]
-    copies = spread(heads, width)
-    fixed = jnp.dot(
-        jnp.concatenate([bias_ref[...], decay_ref[...]], axis=0),
-        copies,
-        precision=lax.Precision.HIGHEST,
-        preferred_element_type=jnp.float32,
-    )
-    step = jnp.dot(
-        past_dt_ref[0], copies.astype(jnp.bfloat16), preferred_element_type=jnp.float32
-    )
-    dt = softplus(step + fixed[0:1])
-    live = lax.broadcasted_iota(jnp.int32, dt.shape, 0) < taken
-    logs = jnp.where(live, -jnp.exp(fixed[1:2]) * dt, 0.0)
-    tails = [jnp.zeros_like(logs[0:1])]
-    for row in range(steps - 1, 0, -1):
-        tails.insert(0, tails[0] + logs[row : row + 1])
-    total = tails[0] + logs[0:1]
-    weight = jnp.where(live, jnp.exp(jnp.concatenate(tails, axis=0)) * dt, 0.0)
-
-    def conv(rows, taps):
-        return sum(taps[k : k + 1] * rows[k : k + steps] for k in range(CONV_W))
-
-    left = weight * silu(conv(past_x_ref[0].astype(jnp.float32), conv_x_ref[...]))
-    right = silu(conv(past_b_ref[0].astype(jnp.float32), conv_b_ref[...]))
-    left_high, left_low = halves_of(left)
-    right_high, right_low = halves_of(right)
-    scale = jnp.exp(total)
-    scale_high, rest = halves_of(scale)
-    scale_mid, rest = halves_of(rest)
-    lhs = jnp.concatenate(
-        [left_high, left_high, left_low, scale_high, scale_mid, rest, jnp.zeros_like(rest)], axis=0
-    ).astype(jnp.bfloat16)
-    rhs = jnp.concatenate([right_high, right_low, right_high], axis=0)
-    rhs = jnp.concatenate([rhs, jnp.zeros((4, rhs.shape[1]), jnp.float32)], axis=0).astype(
-        jnp.bfloat16
-    )
+    each = heads // groups
+
+    @pl.when(pl.program_id(0) == 0)
+    def _():
+        first = 0
+        if step_weight_ref.shape[0] > heads:
+            first = pl.multiple_of(lax.axis_index("tp") * heads, heads)
+        step = lax.dot_general(
+            stacked_rows(rows_ref),
+            step_weight_ref[pl.ds(first, heads), :],
+            (((1,), (1,)), ((), ())),
+            preferred_element_type=jnp.float32,
+        )
+        step_ref[...] = step.astype(jnp.bfloat16)
+        for s in range(count):
+            step_out_ref[s] = step[s * steps : (s + 1) * steps].astype(jnp.bfloat16)
+
+        copies = spread(heads, width)
+        fixed = jnp.dot(
+            jnp.concatenate([bias_ref[...], decay_ref[...]], axis=0),
+            copies,
+            precision=lax.Precision.HIGHEST,
+            preferred_element_type=jnp.float32,
+        )
+        past_dt = jnp.dot(
+            stacked_rows(past_dt_ref),
+            copies.astype(jnp.bfloat16),
+            preferred_element_type=jnp.float32,
+        )
+        dt = softplus(past_dt + fixed[0:1])
+        row = lax.broadcasted_iota(jnp.int32, (tokens, 1), 0)
+        place = row % steps
+        taken = jnp.zeros_like(row)
+        for s in range(count):
+            taken = jnp.where(row // steps == s, taken_ref[s], taken)
+        live = place < taken
+        logs = jnp.where(live, -jnp.exp(fixed[1:2]) * dt, 0.0)
+        tail = jnp.zeros_like(logs)
+        for ahead in range(1, steps):
+            moved = pltpu.roll(logs, tokens - ahead, 0)
+            tail = tail + jnp.where(place + ahead < steps, moved, 0.0)
+        weight = jnp.where(live, jnp.exp(tail) * dt, 0.0)
+        scale = jnp.exp(tail + logs)
+
+        pick = place_in(
+            CONV_W * tokens,
+            past_x_ref.shape[0] * count,
+            lambda r: (r // tokens + r % steps) * count + (r % tokens) // steps,
+        )
+
+        def conv(past_ref, taps_ref):
+            rows = jnp.dot(pick, stacked_rows(past_ref), preferred_element_type=jnp.float32)
+            return silu(
+                sum(
+                    taps_ref[k : k + 1] * rows[k * tokens : (k + 1) * tokens]
+                    for k in range(CONV_W)
+                )
+            )
+
+        left_high, left_low = halves_of(weight * conv(past_x_ref, conv_x_ref))
+        right_high, right_low = halves_of(conv(past_b_ref, conv_b_ref))
+        scale_high, rest = halves_of(scale)
+        scale_mid, rest = halves_of(rest)
+        for s in range(count):
+            all_rows = slice(s * steps, (s + 1) * steps)
+            one = slice(s * steps, s * steps + 1)
+            lhs_ref[s] = jnp.concatenate(
+                [left_high[all_rows], left_high[all_rows], left_low[all_rows]]
+                + [scale_high[one], scale_mid[one], rest[one], jnp.zeros_like(rest[one])],
+                axis=0,
+            ).astype(jnp.bfloat16)
+            rhs_ref[s] = jnp.concatenate(
+                [right_high[all_rows], right_low[all_rows], right_high[all_rows]]
+                + [jnp.zeros((4, rhs_ref.shape[2]), jnp.float32)],
+                axis=0,
+            ).astype(jnp.bfloat16)
+
+    lhs, rhs = lhs_ref[pl.program_id(0)], rhs_ref[pl.program_id(0)]
     row = lax.broadcasted_iota(jnp.int32, (3 * steps + 4, states), 0)
     ones = jnp.where((row >= 3 * steps) & (row < 3 * steps + 3), 1.0, 0.0).astype(jnp.bfloat16)
-    each = heads // groups
     for group in range(groups):
         both = lax.dot_general(
             lhs[:, group * span : (group + 1) * span],
@@ -178,37 +257,49 @@
         base = base_ref[0, group * each : (group + 1) * each].reshape(span, states)
         root = both[:, states:] * base + both[:, :states]
         root_ref[0, group * each : (group + 1) * each] = root.reshape(each, width, states)
-        short_ref[0, group * span : (group + 1) * span] = root.astype(jnp.bfloat16)
-
-
-def make_root(base, past_x, past_b, past_dt, taken, conv_x, conv_b, bias, decay):
+        rows = slice(group * span, (group + 1) * span)
+        short_ref[pl.program_id(0), rows] = root.astype(jnp.bfloat16)
+
+
+def make_root(base, past_x, past_b, past_dt, taken, conv_x, conv_b, bias, decay, rows, step_weight):
     count, heads, width, states = base.shape
+    steps = past_dt.shape[1]
 
     def one(*dims):
         return pl.BlockSpec((1,) + dims, lambda s: (s,) + (0,) * len(dims))
 
-    def same(item):
-        return pl.BlockSpec(item.shape, lambda s: (0,) * item.ndim)
-
-    args = (past_x, past_b, past_dt)
-    fixed = (conv_x, conv_b, bias[None], decay[None])
+    def same(*dims):
+        return pl.BlockSpec(dims, lambda s: (0,) * len(dims))
+
+    fixed = (past_x, past_b, past_dt, conv_x, conv_b, bias[None], decay[None], rows, step_weight)
+    depth = 3 * steps + 4
     return pl.pallas_call(
         root_kernel,
         grid=(count,),
         in_specs=[pl.BlockSpec(memory_space=pltpu.SMEM), one(*base.shape[1:])]
-        + [one(*item.shape[1:]) for item in args]
-        + [same(item) for item in fixed],
-        out_specs=[one(*base.shape[1:]), one(heads * width, states)],
+        + [same(*item.shape) for item in fixed],
+        out_specs=[
+            one(*base.shape[1:]),
+            pl.BlockSpec(memory_space=pltpu.VMEM),
+            same(count * steps, heads),
+            same(count, steps, heads),
+        ],
         out_shape=[
             jax.ShapeDtypeStruct(base.shape, jnp.float32),
-            jax.ShapeDtypeStruct((count, heads * width, states), jnp.bfloat16),
+            pltpu.VMEM((count, heads * width, states), jnp.bfloat16),
+            jax.ShapeDtypeStruct((count * steps, heads), jnp.bfloat16),
+            jax.ShapeDtypeStruct((count, steps, heads), jnp.bfloat16),
+        ],
+        scratch_shapes=[
+            pltpu.VMEM((count, depth, heads * width), jnp.bfloat16),
+            pltpu.VMEM((count, depth, past_b.shape[2]), jnp.bfloat16),
         ],
         cost_estimate=pl.CostEstimate(
             flops=4 * base.size * 16, bytes_accessed=10 * base.size, transcendentals=0
         ),
         compiler_params=grant(16),
         name="root",
-    )(taken, base, *args, *fixed)
+    )(taken, *[apart(item) for item in (base, *fixed)])
 
 
 def mixer_kernel(
@@ -239,7 +330,7 @@
     rows_c_ref,
     sems,
 ):
-    count, kept, channels = past_x_ref.shape
+    kept, count, channels = past_x_ref.shape
     tokens = step_ref.shape[0]
     steps = tokens // count
     heads = bias_ref.shape[1]
@@ -260,8 +351,6 @@
             first = starts[kind] + block * spans[kind]
             now_ref[:, first : first + spans[kind]] = total.astype(jnp.bfloat16)
 
-    stride = kept + 1
-
     def pick(rows, source_of, columns):
         row = lax.broadcasted_iota(jnp.int32, (rows, columns), 0)
         column = lax.broadcasted_iota(jnp.int32, (rows, columns), 1)
@@ -272,7 +361,7 @@
         for s in range(count):
             place, seq = window_place(row)
             hit = (seq == s) & (place < CONV_W - 1)
-            found = found | (hit & (column == s * stride + taken_ref[s] + place))
+            found = found | (hit & (column == (taken_ref[s] + place) * count + s))
         return jnp.where(found, 1.0, 0.0).astype(jnp.bfloat16)
 
     def from_now(row, column):
@@ -290,22 +379,14 @@
         return place, seq
 
     rows = CONV_W * tokens + count * kept
-    pick_past = pick(rows, from_past, count * stride)
+    pick_past = pick(rows, from_past, kept * count)
     pick_now = pick(rows, from_now, tokens)
 
     moves = []
 
     def window(past_ref, first, taps_ref, next_ref, rows_ref):
         size = past_ref.shape[2]
-        past = jnp.concatenate(
-            [
-                jnp.concatenate(
-                    [past_ref[s].astype(jnp.float32), jnp.zeros((1, size), jnp.float32)], axis=0
-                )
-                for s in range(count)
-            ],
-            axis=0,
-        ).astype(jnp.bfloat16)
+        past = stacked_rows(past_ref)
         picked = jnp.dot(pick_past, past, preferred_element_type=jnp.float32) + jnp.dot(
             pick_now, now_ref[:, first : first + size], preferred_element_type=jnp.float32
         )
@@ -390,7 +471,8 @@
 
 def make_mixer(outer, inner, spans, taken, parts, short, step, pasts, convs, vectors):
     tokens = step.shape[0]
-    args = (close(parts), short, step) + pasts + convs + tuple(item[None] for item in vectors)
+    small = (step, *pasts, *convs, *[item[None] for item in vectors])
+    args = (close(parts), close(short), *[apart(item) for item in small])
     channels = pasts[0].shape[2]
     vmem = pl.BlockSpec(memory_space=pltpu.VMEM)
     return pl.pallas_call(
@@ -398,11 +480,11 @@
         in_specs=[pl.BlockSpec(memory_space=pltpu.SMEM)] + [vmem] * len(args),
         out_specs=[vmem] + [pl.BlockSpec(memory_space=pltpu.HBM)] * 3,
         out_shape=[pltpu.VMEM((tokens, channels), jnp.bfloat16)]
-        + [jax.ShapeDtypeStruct(turned(item), jnp.bfloat16) for item in pasts],
+        + [jax.ShapeDtypeStruct(item.shape, jnp.bfloat16) for item in pasts],
         scratch_shapes=[
             pltpu.VMEM((tokens, sum(item.shape[2] for item in pasts) + channels), jnp.bfloat16)
         ]
-        + [pltpu.VMEM(turned(item), jnp.bfloat16) for item in pasts]
+        + [pltpu.VMEM(item.shape, jnp.bfloat16) for item in pasts]
         + [pltpu.SemaphoreType.DMA((3,))],
         cost_estimate=pl.CostEstimate(
             flops=4 * short.size * tokens, bytes_accessed=2 * short.size, transcendentals=0
@@ -412,23 +494,33 @@
     )(taken, *args)
 
 
-def product_kernel(outer, inner, *refs):
-    ys, columns, out_ref = refs[:outer], refs[outer : outer + inner], refs[outer + inner]
+def product_kernel(outer, chunks, *refs):
+    ys, columns, out_ref = refs[:outer], refs[outer:-1], refs[-1]
     stacked = jnp.concatenate([item[...] for item in ys], axis=0)
-    size = columns[0].shape[1]
-    for step in range(inner):
-        result = jnp.dot(stacked, columns[step][...], preferred_element_type=jnp.float32)
-        out_ref[:, step * size : (step + 1) * size] = result.astype(jnp.bfloat16)
+    size, at = columns[0].shape[1], 0
+    for step, count in enumerate(chunks):
+        total, row = None, 0
+        for ref in columns[at : at + count]:
+            term = jnp.dot(
+                stacked[:, row : row + ref.shape[0]],
+                ref[...],
+                preferred_element_type=jnp.float32,
+            )
+            total = term if total is None else total + term
+            row = row + ref.shape[0]
+        out_ref[:, step * size : (step + 1) * size] = total.astype(jnp.bfloat16)
+        at = at + count
 
 
 def make_product(ys, columns):
     outer, inner = len(ys), len(columns)
     tokens, depth = ys[0].shape
-    size = columns[0].shape[1]
+    size = columns[0][0].shape[1]
     vmem = pl.BlockSpec(memory_space=pltpu.VMEM)
+    items = [*ys, *[chunk for item in columns for chunk in item]]
     return pl.pallas_call(
-        functools.partial(product_kernel, outer, inner),
-        in_specs=[vmem] * (outer + inner),
+        functools.partial(product_kernel, outer, tuple(len(item) for item in columns)),
+        in_specs=[vmem] * len(items),
         out_specs=vmem,
         out_shape=pltpu.VMEM((outer * tokens, inner * size), jnp.bfloat16),
         cost_estimate=pl.CostEstimate(
@@ -438,7 +530,7 @@
         ),
         compiler_params=grant(6),
         name="product",
-    )(*[close(item) for item in (*ys, *columns)])
+    )(*[close(item) for item in items])
 
 
 def join_kernel(left_ref, right_ref, *outs):
@@ -462,41 +554,45 @@
     )(close(left), close(right))
 
 
-def arrange_kernel(outer, inner, *refs):
-    out_ref = refs[outer]
+def arrange_kernel(outs, ins, ranks, *refs):
+    out_ref = refs[len(outs)]
     count, steps, _ = out_ref.shape
-    size = refs[0].shape[1] // inner
-    half = outer // 2
+    size = refs[0].shape[1] // len(ins)
+    half = ranks // 2
     me, side = lax.axis_index("kv"), lax.axis_index("tp")
-    me_outer, me_inner = lax.div(me, inner), lax.rem(me, inner)
-    for step in range(outer):
-        shard = me_outer ^ step
-
-        @pl.when(lax.div(shard, half) == side)
-        def _(step=step, shard=shard):
-            item = refs[step][...].astype(jnp.float32)
-            for sub in range(inner):
-                column = (lax.rem(shard, half) * inner + (me_inner ^ sub)) * size
+    for place, out in enumerate(outs):
+
+        @pl.when(lax.div(me ^ out, half) == side)
+        def _(place=place, out=out):
+            item = refs[place][...].astype(jnp.float32)
+            for sub, step in enumerate(ins):
+                column = lax.rem(me ^ (out ^ step), half) * size
                 column = pl.multiple_of(column, size)
                 for s in range(count):
                     block = item[s * steps : (s + 1) * steps, sub * size : (sub + 1) * size]
                     out_ref[s, :, pl.ds(column, size)] = block.astype(jnp.bfloat16)
 
 
-def make_arranged(items, inner, count):
-    outer = len(items)
+def make_arranged(items, outs, ins, ranks, count):
     tokens, columns = items[0].shape
     vmem = pl.BlockSpec(memory_space=pltpu.VMEM)
     return pl.pallas_call(
-        functools.partial(arrange_kernel, outer, inner),
-        in_specs=[vmem] * outer,
+        functools.partial(arrange_kernel, outs, ins, ranks),
+        in_specs=[vmem] * len(outs),
         out_specs=vmem,
         out_shape=jax.ShapeDtypeStruct(
-            (count, tokens // count, outer // 2 * columns), jnp.bfloat16
+            (count, tokens // count, len(outs) // 2 * columns), jnp.bfloat16
         ),
         compiler_params=grant(2),
         name="arrange",
     )(*[close(item) for item in items])
+
+
+def sums_of(bits):
+    found = [0]
+    for bit in bits:
+        found = found + [item | bit for item in found]
+    return tuple(found)
 
 
 def inner_size(ranks):
@@ -541,7 +637,6 @@
     inner = inner_size(ranks)
     outer = ranks // inner
     me_inner = lax.rem(me, inner)
-    me_outer = lax.div(me, inner)
 
     weights = (gate_weight, value_weight, write_weight, read_weight)
     spans = [item.shape[1] // inner for item in weights]
@@ -573,9 +668,6 @@
     flat = normed.reshape(seq_local * proposals, width)
     token_count = flat.shape[0]
     head_count = step_bias.shape[0]
-    own_step = lax.dynamic_slice_in_dim(step_weight, side * head_count, head_count, 1)
-    step_now = jnp.dot(flat, own_step, preferred_element_type=jnp.float32).astype(jnp.bfloat16)
-
     part = width // (outer * halves)
     share = lax.dynamic_index_in_dim(
         flat.reshape(token_count, outer, halves, part), side, 2, keepdims=False
@@ -600,9 +692,20 @@
     else:
         product = make_partial(everyone, narrow)
     returned = lax.all_to_all(product, "kv", split_axis=0, concat_axis=0, tiled=True)
-    columns = [out_weight]
-    for step in range(1, inner):
-        columns.append(swap(out_weight, step))
+    bits = [1 << k for k in range(ranks.bit_length() - 1)]
+    ins, outs = sums_of(bits[0::2]), sums_of(bits[1::2])
+    columns = [[out_weight]]
+    if len(ins) == 4:
+        near_bit, far_bit = bits[0], bits[2]
+        far = swap(out_weight, far_bit)
+        beside = swap(out_weight, near_bit)
+        cut = out_weight.shape[0] // 2
+        first = swap(far[:cut], near_bit)
+        second = swap(beside[cut:], far_bit)
+        columns = [[make_held(out_weight)], [beside], [far], [first, second]]
+    else:
+        for step in ins[1:]:
+            columns.append([swap(out_weight, step)])
     returned = returned.reshape(ranks, token_count, sum(spans))
     shards, pieces = outer, inner
     if any(span % 128 for span in spans):
@@ -618,7 +721,13 @@
         spans = [inner * span for span in spans]
         shards, pieces = 1, 1
 
-    root_state, short = make_root(
+    past_value, past_write, past_read = [
+        jnp.swapaxes(item, 0, 1) for item in (past_value, past_write, past_read)
+    ]
+    turned = jnp.swapaxes(step_weight, 0, 1)
+    if head_count % 16:
+        turned = lax.dynamic_slice_in_dim(turned, side * head_count, head_count, 0)
+    root_state, short, step_now, step_out = make_root(
         base_state,
         past_value,
         past_write,
@@ -628,6 +737,8 @@
         conv_write,
         step_bias,
         decay_log,
+        normed,
+        turned,
     )
     flat_y, *nexts = make_mixer(
         shards,
@@ -642,39 +753,30 @@
         (step_bias, decay_log, skip_gain, output_gain),
     )
     next_value, next_write, next_read = [jnp.swapaxes(item, 0, 1) for item in nexts]
-    ys = [flat_y] + [swap(flat_y, inner * step) for step in range(1, outer)]
-    step_out = step_now.reshape(seq_local, proposals, head_count)
-    if out_weight.shape[1] % 128 == 0 and halves == 2 and outer % 2 == 0:
+    ys = [flat_y] + [swap(flat_y, step) for step in outs[1:]]
+    if out_weight.shape[1] % 128 == 0 and halves == 2 and bits[-1] in outs:
         partial = make_product(ys, columns)
-        keeper = [(k // inner) // (outer // 2) for k in range(ranks)]
+        keeper = [k // (ranks // 2) for k in range(ranks)]
         other = lax.ppermute(
             partial, ("kv", "tp"), [(2 * k + 1 - keeper[k], 2 * k + keeper[k]) for k in range(ranks)]
         )
-        sums = make_joined(partial, other, outer)
-        blocks = [sums[0]] + [
-            lax.ppermute(
-                sums[step],
-                ("kv", "tp"),
-                [(2 * k + keeper[k], 2 * (k ^ (inner * step)) + keeper[k]) for k in range(ranks)],
-            )
-            for step in range(1, outer)
-        ]
-        mixed = make_arranged(blocks, inner, seq_local)
+        sums = make_joined(partial, other, len(outs))
+        blocks = [sums[0]]
+        for place, step in enumerate(outs[1:], 1):
+            pairs = [(2 * k + keeper[k], 2 * (k ^ step) + keeper[k]) for k in range(ranks)]
+            blocks.append(lax.ppermute(sums[place], ("kv", "tp"), pairs))
+        mixed = make_arranged(blocks, outs, ins, ranks, seq_local)
         return (mixed, root_state, next_value, next_write, next_read, step_out)
     stacked = jnp.concatenate(ys, axis=0)
-    partial = jnp.concatenate(
-        [
-            jnp.dot(stacked, item, preferred_element_type=jnp.float32).astype(jnp.bfloat16)
-            for item in columns
-        ],
-        axis=1,
-    ).reshape(outer, token_count, -1)
-    blocks = jnp.stack(
-        [partial[0]] + [swap(partial[step], inner * step) for step in range(1, outer)]
-    ).reshape(outer, token_count, inner, -1)
-    order_outer = me_outer ^ jnp.arange(outer)
-    order_inner = me_inner ^ jnp.arange(inner)
-    blocks = jnp.take(jnp.take(blocks, order_outer, axis=0), order_inner, axis=2)
+    blocks = {}
+    for step, chunks in zip(ins, columns):
+        item = jnp.concatenate(chunks, axis=0)
+        product = jnp.dot(stacked, item, preferred_element_type=jnp.float32)
+        product = product.astype(jnp.bfloat16).reshape(len(outs), token_count, -1)
+        for place, out in enumerate(outs):
+            blocks[out ^ step] = swap(product[place], out) if out else product[place]
+    blocks = jnp.stack([blocks[step] for step in range(ranks)])
+    blocks = jnp.take(blocks, me ^ jnp.arange(ranks), axis=0)
     full = jnp.swapaxes(blocks, 0, 1).reshape(token_count, halves, width // halves)
     shares = lax.all_to_all(full, "tp", split_axis=1, concat_axis=1, tiled=True)
     mixed = jnp.sum(shares.astype(jnp.float32), axis=1).astype(jnp.bfloat16)

time: 79.9 us -> 93.6 us (1.17)
  the two profiles are of different devices: /device:TPU:0 before, /device:TPU:1 now
where the time goes in v1:
time: 93.6 us; the launch traced here: 93 us
  waiting for transfers between devices  32.4 us (35%)
  starting transfers between devices  21.5 us (23%)
  blocking collectives  19.8 us (21%)
  Pallas kernels  15.3 us (16%)
  local copies, waits for them, and re-layouts  2.25 us (2%)
  other arithmetic  0.94 us (1%)
    ppermute x10, waiting for transfers between devices, swap(): return lax.ppermute(item, 'kv', [(k, k ^ step) for k in range(ranks)])  26.5 us
    all_to_all x1, blocking collectives, whole_step(): lax.all_to_all(share, 'kv', split_axis=0, concat_axis=0, tiled=True)  13.5 us
    ppermute x10, starting transfers between devices, swap(): return lax.ppermute(item, 'kv', [(k, k ^ step) for k in range(ranks)])  10.9 us
    pallas_call x1, Pallas kernels, make_root(): pl.pallas_call(root_kernel, grid=(count,), in_specs=[pl.BlockSpec(memory_...  6.6 us
    ppermute x3, waiting for transfers between devices, whole_step(): blocks.append(lax.ppermute(sums[place], ('kv', 'tp'), pairs))  4.97 us
    ppermute x1, starting transfers between devices, whole_step(): lax.ppermute(partial, ('kv', 'tp'), [(2 * k + 1 - keeper[k], 2 * k + keep...  3.76 us
    all_to_all x1, starting transfers between devices, whole_step(): lax.all_to_all(product, 'kv', split_axis=0, concat_axis=0, tiled=True)  3.62 us
    all_gather x1, blocking collectives, whole_step(): everyone = lax.all_gather(everyone, 'tp', axis=1, tiled=True)  3.4 us
  transfers between devices with their start and end apart: 15, of which 6 were waited for; matrix products, arithmetic and copies ran while one was open for 3% of the time, Pallas kernels for 11%

profile of v1, /device:TPU:1, one launch (start us, length us, event | category | flops | bytes accessed | tf_op | source)
XLA Modules:
  0.0 93.0 jit_solution(3858045919083596692)
XLA Ops:
  0.6 0.0 copy-start.3
  0.6 1.5 %pack.1 = (bf16[128,1280]{1,0:T(8,128)(2,1)S(1)}, bf16[128,1280]{1,0:T(8,128)(2,1)S(1)}, bf16[128,1280]{1,0:T(8,128)(2,1)S(1)}, bf16[128,1280]{1,0:T(8,128)(2,1)S(1)}) custom-call(bf16[128,2048]{1,0:T(8,128)(2,1)} %gate_ref.1, bf16[128,2048]{1,0:T(8,128)(2,1)} %value_ref.1, bf16[128,512]{1,0:T(8,128)(2,1)} %write_ref.1, bf16[128,512]{1,0:T(8,128)(2,1)} %read_ref.1), custom_call_target="tpu_custom_call" | custom-call | tf_op jit(solution)/shard_map/pack/pallas_call | solution.py:71
  2.2 2.1 %collective-permute-start = (bf16[128,1280]{1,0:T(8,128)(2,1)S(1)}, bf16[128,1280]{1,0:T(8,128)(2,1)S(1)}, u32[]{:S(2)}, u32[]{:S(2)}) collective-permute-start(bf16[128,1280]{1,0:T(8,128)(2,1)S(1)} %get-tuple-element.23), channel_id=1, source_target_pairs={{0,2},{2,0},{4,6},{6,4},{8,10},{10,8},{12,14},{14,12},{16,18},{18,... | collective-permute-start | bytes 983048 | tf_op jit(solution)/shard_map/ppermute | solution.py:607
  4.3 1.2 %collective-permute-start.1 = (bf16[128,1280]{1,0:T(8,128)(2,1)S(1)}, bf16[128,1280]{1,0:T(8,128)(2,1)S(1)}, u32[]{:S(2)}, u32[]{:S(2)}) collective-permute-start(bf16[128,1280]{1,0:T(8,128)(2,1)S(1)} %get-tuple-element.24), channel_id=1, source_target_pairs={{0,4},{2,6},{4,0},{6,2},{8,12},{10,14},{12,8},{14,10},{16,20},{18,... | collective-permute-start | bytes 983048 | tf_op jit(solution)/shard_map/ppermute | solution.py:607
  5.5 0.0 collective-permute-start.2
  5.5 2.9 %all_gather.6 = bf16[4,4,2048]{2,1,0:T(4,128)(2,1)S(1)} all-gather(bf16[4,4,1024]{2,1,0:T(4,128)(2,1)} %param.21), channel_id=1, replica_groups=mesh['kv'=16,'tp'=2] {'tp'}, dimensions={2}, use_global_device_ids=true | all-gather | bytes 98304 | tf_op jit(solution)/shard_map/all_gather | solution.py:662
  8.5 0.1 fusion
  8.6 0.8 fusion.2.rows_ref
  9.4 0.0 copy-start.4
  9.5 0.1 constant_dynamic-slice_fusion
  9.6 13.5 %all_to_all.21 = bf16[16,16,256]{2,1,0:T(8,128)(2,1)S(1)} all-to-all(bf16[16,16,256]{2,1,0:T(8,128)(2,1)S(1)} %bitcast.20), channel_id=1, replica_groups=mesh['kv'=16,'tp'=2] {'kv'}, dimensions={0} | all-to-all | bytes 262144 | tf_op jit(solution)/shard_map/all_to_all | solution.py:678
  23.1 3.4 %all_gather.7.rows_ref = bf16[256,512]{1,0:T(8,128)(2,1)S(1)} all-gather(bf16[256,256]{1,0:T(8,128)(2,1)S(1)} %bitcast.19), channel_id=1, replica_groups=mesh['kv'=16,'tp'=2] {'tp'}, dimensions={1}, use_global_device_ids=true | all-gather | bytes 393216 | tf_op jit(solution)/shard_map/all_gather | solution.py:679
  26.5 0.0 collective-permute-done.refs_1_
  26.5 0.0 collective-permute-done.1.refs_2_
  26.5 0.0 collective-permute-done.2.refs_3_
  26.5 1.7 %partial.1 = bf16[256,1280]{1,0:T(8,128)(2,1)} custom-call(bf16[256,512]{1,0:T(8,128)(2,1)S(1)} %all_gather.7.rows_ref, bf16[128,1280]{1,0:T(8,128)(2,1)S(1)} %get-tuple-element.22.refs_0_, bf16[128,1280]{1,0:T(8,128)(2,1)S(1)} %collective-permute-done.refs_1_, bf16[128,1280]{1,0:T(8,128)(2,1)S(1)} %collective-permute-done.1.refs_2_, ...), custom_call_target="tpu_custom_call" | custom-call | flops 335544320 | bytes 655360 | tf_op jit(solution)/shard_map/partial/pallas_call | solution.py:101
  28.2 3.6 %all-to-all-start.1 = ((bf16[16,16,1280]{2,1,0:T(8,128)(2,1)}), bf16[16,16,1280]{2,1,0:T(8,128)(2,1)S(1)}, u32[]{:S(2)}, u32[]{:S(2)}) async-start(bf16[16,16,1280]{2,1,0:T(8,128)(2,1)} %bitcast.4), calls=%async_computation.1 | async-start | bytes 1310720 | tf_op jit(solution)/shard_map/all_to_all | solution.py:694
  31.8 1.4 %collective-permute-start.7 = (bf16[2048,128]{1,0:T(8,128)(2,1)}, bf16[2048,128]{1,0:T(8,128)(2,1)S(1)}, u32[]{:S(2)}, u32[]{:S(2)}) collective-permute-start(bf16[2048,128]{1,0:T(8,128)(2,1)} %from_ref.1), channel_id=1, source_target_pairs={{0,8},{2,10},{4,12},{6,14},{8,0},{10,2},{12,4},{14,6},{16,24},{18,... | collective-permute-start | bytes 1572872 | tf_op jit(solution)/shard_map/ppermute | solution.py:607
  33.2 1.2 %collective-permute-start.6 = (bf16[2048,128]{1,0:T(8,128)(2,1)}, bf16[2048,128]{1,0:T(8,128)(2,1)S(1)}, u32[]{:S(2)}, u32[]{:S(2)}) collective-permute-start(bf16[2048,128]{1,0:T(8,128)(2,1)} %from_ref.1), channel_id=1, source_target_pairs={{0,2},{2,0},{4,6},{6,4},{8,10},{10,8},{12,14},{14,12},{16,18},{18,... | collective-permute-start | bytes 1572872 | tf_op jit(solution)/shard_map/ppermute | solution.py:607
  34.4 21.0 %collective-permute-done.7.refs_6_ = bf16[2048,128]{1,0:T(8,128)(2,1)S(1)} collective-permute-done((bf16[2048,128]{1,0:T(8,128)(2,1)}, bf16[2048,128]{1,0:T(8,128)(2,1)S(1)}, u32[]{:S(2)}, u32[]{:S(2)}) %collective-permute-start.7) | collective-permute-done | bytes 524320 | tf_op jit(solution)/shard_map/ppermute | solution.py:607
  55.4 0.7 slice.8
  56.1 1.2 %collective-permute-start.8 = (bf16[1024,128]{1,0:T(8,128)(2,1)}, bf16[1024,128]{1,0:T(8,128)(2,1)S(1)}, u32[]{:S(2)}, u32[]{:S(2)}) collective-permute-start(bf16[1024,128]{1,0:T(8,128)(2,1)} %slice.8), channel_id=1, source_target_pairs={{0,2},{2,0},{4,6},{6,4},{8,10},{10,8},{12,14},{14,12},{16,18},{18,... | collective-permute-start | bytes 786440 | tf_op jit(solution)/shard_map/ppermute | solution.py:607
  57.3 0.0 collective-permute-done.6.refs_5_
  57.3 0.8 slice.9
  58.1 0.2 collective-permute-start.9
  58.3 6.6 %root.1 = (f32[4,32,64,128]{3,2,1,0:T(8,128)}, bf16[4,2048,128]{2,1,0:T(8,128)(2,1)S(1)}, bf16[16,32]{1,0:T(8,128)(2,1)S(1)}, bf16[4,4,32]{2,1,0:T(4,128)(2,1)}) custom-call(s32[4]{0:T(128)S(1)} %copy-done.3, f32[4,32,64,128]{3,2,1,0:T(8,128)} %base_ref.1, bf16[7,4,2048]{2,1,0:T(4,128)(2,1)} %bitcast.21, bf16[7,4,512]{2,1,0:T(4,128)(2,1)} %bitcast.25, ...), custom_call_target="tpu_custom_call" | custom-call | flops 67108864 | bytes 10485760 | tf_op jit(solution)/shard_map/root/pallas_call | solution.py:276
  64.9 0.6 copy-done.2
  65.5 0.0 all-to-all-done.1.parts_ref
  65.5 2.4 %mixer.1 = (bf16[16,2048]{1,0:T(8,128)(2,1)S(1)}, bf16[7,4,2048]{2,1,0:T(4,128)(2,1)}, bf16[7,4,512]{2,1,0:T(4,128)(2,1)}, bf16[7,4,512]{2,1,0:T(4,128)(2,1)}) custom-call(s32[4]{0:T(128)S(1)} %copy-done.3, bf16[16,16,1280]{2,1,0:T(8,128)(2,1)S(1)} %all-to-all-done.1.parts_ref, bf16[4,2048,128]{2,1,0:T(8,128)(2,1)S(1)} %get-tuple-element.26.short_ref, ...), custom_call_target="tpu_custom_call" | custom-call | flops 67108864 | bytes 2097152 | tf_op jit(solution)/shard_map/mixer/pallas_call | solution.py:478
  67.9 1.2 %collective-permute-start.3 = (bf16[16,2048]{1,0:T(8,128)(2,1)S(1)}, bf16[16,2048]{1,0:T(8,128)(2,1)S(1)}, u32[]{:S(2)}, u32[]{:S(2)}) collective-permute-start(bf16[16,2048]{1,0:T(8,128)(2,1)S(1)} %get-tuple-element.28.refs_0_), channel_id=1, source_target_pairs={{0,4},{2,6},{4,0},{6,2},{8,12},{10,14},{12,8},{14,10},{16,20},{18,... | collective-permute-start | bytes 196616 | tf_op jit(solution)/shard_map/ppermute | solution.py:607
  69.1 2.2 %collective-permute-start.4 = (bf16[16,2048]{1,0:T(8,128)(2,1)S(1)}, bf16[16,2048]{1,0:T(8,128)(2,1)S(1)}, u32[]{:S(2)}, u32[]{:S(2)}) collective-permute-start(bf16[16,2048]{1,0:T(8,128)(2,1)S(1)} %get-tuple-element.28.refs_0_), channel_id=1, source_target_pairs={{0,16},{2,18},{4,20},{6,22},{8,24},{10,26},{12,28},{14,30},{16,0},... | collective-permute-start | bytes 196616 | tf_op jit(solution)/shard_map/ppermute | solution.py:607
  71.3 0.2 collective-permute-start.5
  71.5 1.0 %hold.1.refs_4_ = bf16[2048,128]{1,0:T(8,128)(2,1)S(1)} custom-call(bf16[2048,128]{1,0:T(8,128)(2,1)} %from_ref.1), custom_call_target="tpu_custom_call" | custom-call | flops 16777216 | bytes 1048576 | tf_op jit(solution)/shard_map/hold/pallas_call | solution.py:121
  72.5 0.0 collective-permute-done.8.refs_7_
  72.6 0.0 collective-permute-done.9.refs_8_
  72.6 0.0 collective-permute-done.3.refs_1_
  72.6 0.6 collective-permute-done.4.refs_2_
  73.1 4.9 %collective-permute-done.5.refs_3_ = bf16[16,2048]{1,0:T(8,128)(2,1)S(1)} collective-permute-done((bf16[16,2048]{1,0:T(8,128)(2,1)S(1)}, bf16[16,2048]{1,0:T(8,128)(2,1)S(1)}, u32[]{:S(2)}, u32[]{:S(2)}) %collective-permute-start.5) | collective-permute-done | bytes 65568 | tf_op jit(solution)/shard_map/ppermute | solution.py:607
  78.0 1.4 %product.1.left_ref = bf16[64,512]{1,0:T(8,128)(2,1)S(1)} custom-call(bf16[16,2048]{1,0:T(8,128)(2,1)S(1)} %get-tuple-element.28.refs_0_, bf16[16,2048]{1,0:T(8,128)(2,1)S(1)} %collective-permute-done.3.refs_1_, bf16[16,2048]{1,0:T(8,128)(2,1)S(1)} %collective-permute-done.4.refs_2_, bf16[16,2048]{1,0:T(8,128)(2,1)S(1)} %collective-permute-done.5.refs_3_, ...), custom_call_target="tpu_custom_call" | custom-call | flops 134217728 | bytes 2097152 | tf_op jit(solution)/shard_map/product/pallas_call | solution.py:521
  79.5 3.8 %collective-permute-start.10 = (bf16[64,512]{1,0:T(8,128)(2,1)S(1)}, bf16[64,512]{1,0:T(8,128)(2,1)S(1)}, u32[]{:S(2)}, u32[]{:S(2)}) collective-permute-start(bf16[64,512]{1,0:T(8,128)(2,1)S(1)} %product.1.left_ref), channel_id=1, source_target_pairs={{1,0},{3,2},{5,4},{7,6},{9,8},{11,10},{13,12},{15,14},{16,17},{18,... | collective-permute-start | bytes 196616 | tf_op jit(solution)/shard_map/ppermute | solution.py:760
  83.2 0.9 collective-permute-done.10.right_ref
  84.1 0.7 collective-permute-start.11
  84.8 1.3 %collective-permute-start.12 = (bf16[16,512]{1,0:T(8,128)(2,1)S(1)}, bf16[16,512]{1,0:T(8,128)(2,1)S(1)}, u32[]{:S(2)}, u32[]{:S(2)}) collective-permute-start(bf16[16,512]{1,0:T(8,128)(2,1)S(1)} %get-tuple-element.31), channel_id=1, source_target_pairs={{0,16},{2,18},{4,20},{6,22},{8,24},{10,26},{12,28},{14,30},{17,1},... | collective-permute-start | bytes 49160 | tf_op jit(solution)/shard_map/ppermute | solution.py:767
  86.1 1.3 %collective-permute-start.13 = (bf16[16,512]{1,0:T(8,128)(2,1)S(1)}, bf16[16,512]{1,0:T(8,128)(2,1)S(1)}, u32[]{:S(2)}, u32[]{:S(2)}) collective-permute-start(bf16[16,512]{1,0:T(8,128)(2,1)S(1)} %get-tuple-element.32), channel_id=1, source_target_pairs={{0,20},{2,22},{4,16},{6,18},{8,28},{10,30},{12,24},{14,26},{17,5},... | collective-permute-start | bytes 49160 | tf_op jit(solution)/shard_map/ppermute | solution.py:767
  87.4 0.0 collective-permute-done.11.refs_1_
  87.4 2.8 %collective-permute-done.12.refs_2_ = bf16[16,512]{1,0:T(8,128)(2,1)S(1)} collective-permute-done((bf16[16,512]{1,0:T(8,128)(2,1)S(1)}, bf16[16,512]{1,0:T(8,128)(2,1)S(1)}, u32[]{:S(2)}, u32[]{:S(2)}) %collective-permute-start.12) | collective-permute-done | bytes 16416 | tf_op jit(solution)/shard_map/ppermute | solution.py:767
  90.2 2.2 %collective-permute-done.13.refs_3_ = bf16[16,512]{1,0:T(8,128)(2,1)S(1)} collective-permute-done((bf16[16,512]{1,0:T(8,128)(2,1)S(1)}, bf16[16,512]{1,0:T(8,128)(2,1)S(1)}, u32[]{:S(2)}, u32[]{:S(2)}) %collective-permute-start.13) | collective-permute-done | bytes 16416 | tf_op jit(solution)/shard_map/ppermute | solution.py:767
  92.4 0.6 arrange.1
  (12 shorter events, 0.1 us)
Async XLA Ops:
  0.6 57.7 %copy-start.3 = (s32[4]{0:T(128)S(1)}, s32[4]{0:T(128)}, u32[]{:S(2)}) copy-start(s32[4]{0:T(128)} %taken_ref.3) | copy-start | bytes 52
  2.2 24.3 %collective-permute-start = (bf16[128,1280]{1,0:T(8,128)(2,1)S(1)}, bf16[128,1280]{1,0:T(8,128)(2,1)S(1)}, u32[]{:S(2)}, u32[]{:S(2)}) collective-permute-start(bf16[128,1280]{1,0:T(8,128)(2,1)S(1)} %get-tuple-element.23), channel_id=1, source_target_pairs={{0,2},{2,0},{4,6},{6,4},{8,10},{10,8},{12,14},{14,12},{16,18},{18,... | collective-permute-start | bytes 983048 | tf_op jit(solution)/shard_map/ppermute | solution.py:607
  4.3 22.2 %collective-permute-start.1 = (bf16[128,1280]{1,0:T(8,128)(2,1)S(1)}, bf16[128,1280]{1,0:T(8,128)(2,1)S(1)}, u32[]{:S(2)}, u32[]{:S(2)}) collective-permute-start(bf16[128,1280]{1,0:T(8,128)(2,1)S(1)} %get-tuple-element.24), channel_id=1, source_target_pairs={{0,4},{2,6},{4,0},{6,2},{8,12},{10,14},{12,8},{14,10},{16,20},{18,... | collective-permute-start | bytes 983048 | tf_op jit(solution)/shard_map/ppermute | solution.py:607
  5.5 21.0 %collective-permute-start.2 = (bf16[128,1280]{1,0:T(8,128)(2,1)S(1)}, bf16[128,1280]{1,0:T(8,128)(2,1)S(1)}, u32[]{:S(2)}, u32[]{:S(2)}) collective-permute-start(bf16[128,1280]{1,0:T(8,128)(2,1)S(1)} %get-tuple-element.25), channel_id=1, source_target_pairs={{0,6},{2,4},{4,2},{6,0},{8,14},{10,12},{12,10},{14,8},{16,22},{18,... | collective-permute-start | bytes 983048 | tf_op jit(solution)/shard_map/ppermute | solution.py:607
  9.4 48.9 %copy-start.4 = (bf16[4,4,2048]{2,1,0:T(4,128)(2,1)}, bf16[4,4,2048]{2,1,0:T(4,128)(2,1)S(1)}, u32[]{:S(2)}) copy-start(bf16[4,4,2048]{2,1,0:T(4,128)(2,1)S(1)} %fusion.2.rows_ref) | copy-start | bytes 196612
  28.2 37.3 %all-to-all-start.1 = ((bf16[16,16,1280]{2,1,0:T(8,128)(2,1)}), bf16[16,16,1280]{2,1,0:T(8,128)(2,1)S(1)}, u32[]{:S(2)}, u32[]{:S(2)}) async-start(bf16[16,16,1280]{2,1,0:T(8,128)(2,1)} %bitcast.4), calls=%async_computation.1 | async-start | bytes 1310720 | tf_op jit(solution)/shard_map/all_to_all | solution.py:694
  31.8 23.6 %collective-permute-start.7 = (bf16[2048,128]{1,0:T(8,128)(2,1)}, bf16[2048,128]{1,0:T(8,128)(2,1)S(1)}, u32[]{:S(2)}, u32[]{:S(2)}) collective-permute-start(bf16[2048,128]{1,0:T(8,128)(2,1)} %from_ref.1), channel_id=1, source_target_pairs={{0,8},{2,10},{4,12},{6,14},{8,0},{10,2},{12,4},{14,6},{16,24},{18,... | collective-permute-start | bytes 1572872 | tf_op jit(solution)/shard_map/ppermute | solution.py:607
  33.2 24.1 %collective-permute-start.6 = (bf16[2048,128]{1,0:T(8,128)(2,1)}, bf16[2048,128]{1,0:T(8,128)(2,1)S(1)}, u32[]{:S(2)}, u32[]{:S(2)}) collective-permute-start(bf16[2048,128]{1,0:T(8,128)(2,1)} %from_ref.1), channel_id=1, source_target_pairs={{0,2},{2,0},{4,6},{6,4},{8,10},{10,8},{12,14},{14,12},{16,18},{18,... | collective-permute-start | bytes 1572872 | tf_op jit(solution)/shard_map/ppermute | solution.py:607
  56.1 16.4 %collective-permute-start.8 = (bf16[1024,128]{1,0:T(8,128)(2,1)}, bf16[1024,128]{1,0:T(8,128)(2,1)S(1)}, u32[]{:S(2)}, u32[]{:S(2)}) collective-permute-start(bf16[1024,128]{1,0:T(8,128)(2,1)} %slice.8), channel_id=1, source_target_pairs={{0,2},{2,0},{4,6},{6,4},{8,10},{10,8},{12,14},{14,12},{16,18},{18,... | collective-permute-start | bytes 786440 | tf_op jit(solution)/shard_map/ppermute | solution.py:607
  57.3 1.0 %copy-start = (bf16[2048,128]{1,0:T(8,128)(2,1)}, bf16[2048,128]{1,0:T(8,128)(2,1)S(1)}, u32[]{:S(2)}) copy-start(bf16[2048,128]{1,0:T(8,128)(2,1)S(1)} %collective-permute-done.6.refs_5_) | copy-start | bytes 1572868
  58.1 14.5 %collective-permute-start.9 = (bf16[1024,128]{1,0:T(8,128)(2,1)}, bf16[1024,128]{1,0:T(8,128)(2,1)}, u32[]{:S(2)}, u32[]{:S(2)}) collective-permute-start(bf16[1024,128]{1,0:T(8,128)(2,1)} %slice.9), channel_id=1, source_target_pairs={{0,8},{2,10},{4,12},{6,14},{8,0},{10,2},{12,4},{14,6},{16,24},{18,... | collective-permute-start | bytes 786440 | tf_op jit(solution)/shard_map/ppermute | solution.py:607
  64.9 0.6 copy-start.2
  65.5 12.6 %copy-start.1 = (bf16[2048,128]{1,0:T(8,128)(2,1)S(1)}, bf16[2048,128]{1,0:T(8,128)(2,1)}, u32[]{:S(2)}) copy-start(bf16[2048,128]{1,0:T(8,128)(2,1)} %copy-done) | copy-start | bytes 1572868
  67.9 4.7 %collective-permute-start.3 = (bf16[16,2048]{1,0:T(8,128)(2,1)S(1)}, bf16[16,2048]{1,0:T(8,128)(2,1)S(1)}, u32[]{:S(2)}, u32[]{:S(2)}) collective-permute-start(bf16[16,2048]{1,0:T(8,128)(2,1)S(1)} %get-tuple-element.28.refs_0_), channel_id=1, source_target_pairs={{0,4},{2,6},{4,0},{6,2},{8,12},{10,14},{12,8},{14,10},{16,20},{18,... | collective-permute-start | bytes 196616 | tf_op jit(solution)/shard_map/ppermute | solution.py:607
  69.1 4.0 %collective-permute-start.4 = (bf16[16,2048]{1,0:T(8,128)(2,1)S(1)}, bf16[16,2048]{1,0:T(8,128)(2,1)S(1)}, u32[]{:S(2)}, u32[]{:S(2)}) collective-permute-start(bf16[16,2048]{1,0:T(8,128)(2,1)S(1)} %get-tuple-element.28.refs_0_), channel_id=1, source_target_pairs={{0,16},{2,18},{4,20},{6,22},{8,24},{10,26},{12,28},{14,30},{16,0},... | collective-permute-start | bytes 196616 | tf_op jit(solution)/shard_map/ppermute | solution.py:607
  71.3 6.7 %collective-permute-start.5 = (bf16[16,2048]{1,0:T(8,128)(2,1)S(1)}, bf16[16,2048]{1,0:T(8,128)(2,1)S(1)}, u32[]{:S(2)}, u32[]{:S(2)}) collective-permute-start(bf16[16,2048]{1,0:T(8,128)(2,1)S(1)} %get-tuple-element.28.refs_0_), channel_id=1, source_target_pairs={{0,20},{2,22},{4,16},{6,18},{8,28},{10,30},{12,24},{14,26},{16,4},... | collective-permute-start | bytes 196616 | tf_op jit(solution)/shard_map/ppermute | solution.py:607
  79.5 4.6 %collective-permute-start.10 = (bf16[64,512]{1,0:T(8,128)(2,1)S(1)}, bf16[64,512]{1,0:T(8,128)(2,1)S(1)}, u32[]{:S(2)}, u32[]{:S(2)}) collective-permute-start(bf16[64,512]{1,0:T(8,128)(2,1)S(1)} %product.1.left_ref), channel_id=1, source_target_pairs={{1,0},{3,2},{5,4},{7,6},{9,8},{11,10},{13,12},{15,14},{16,17},{18,... | collective-permute-start | bytes 196616 | tf_op jit(solution)/shard_map/ppermute | solution.py:760
  84.1 3.3 %collective-permute-start.11 = (bf16[16,512]{1,0:T(8,128)(2,1)S(1)}, bf16[16,512]{1,0:T(8,128)(2,1)S(1)}, u32[]{:S(2)}, u32[]{:S(2)}) collective-permute-start(bf16[16,512]{1,0:T(8,128)(2,1)S(1)} %get-tuple-element.30), channel_id=1, source_target_pairs={{0,4},{2,6},{4,0},{6,2},{8,12},{10,14},{12,8},{14,10},{17,21},{19,... | collective-permute-start | bytes 49160 | tf_op jit(solution)/shard_map/ppermute | solution.py:767
  84.8 5.4 %collective-permute-start.12 = (bf16[16,512]{1,0:T(8,128)(2,1)S(1)}, bf16[16,512]{1,0:T(8,128)(2,1)S(1)}, u32[]{:S(2)}, u32[]{:S(2)}) collective-permute-start(bf16[16,512]{1,0:T(8,128)(2,1)S(1)} %get-tuple-element.31), channel_id=1, source_target_pairs={{0,16},{2,18},{4,20},{6,22},{8,24},{10,26},{12,28},{14,30},{17,1},... | collective-permute-start | bytes 49160 | tf_op jit(solution)/shard_map/ppermute | solution.py:767
  86.1 6.3 %collective-permute-start.13 = (bf16[16,512]{1,0:T(8,128)(2,1)S(1)}, bf16[16,512]{1,0:T(8,128)(2,1)S(1)}, u32[]{:S(2)}, u32[]{:S(2)}) collective-permute-start(bf16[16,512]{1,0:T(8,128)(2,1)S(1)} %get-tuple-element.32), channel_id=1, source_target_pairs={{0,20},{2,22},{4,16},{6,18},{8,28},{10,30},{12,24},{14,26},{17,5},... | collective-permute-start | bytes 49160 | tf_op jit(solution)/shard_map/ppermute | solution.py:767
